TPU v7x, 512 devices: a whole 4x4x16 slice. The times are simulated.
512 devices in a mesh: sp: 32 (over z, core), tp: 16 (over y, x).
Axes of the slice: x: 4, y: 4, z: 16, core: 2. Of those that a mesh axis runs over, the one named last changes fastest.
Arguments:
- query_pre: bfloat16 [16384, 2048], P('sp', 'tp'), may hold values from -6 to 6
- forget_pre: bfloat16 [16384, 2048], P('sp', 'tp'), may hold values from -8 to 8
- values_in: bfloat16 [16384, 2048], P('sp', 'tp'), may hold values from -16 to 16
- gate_pre: bfloat16 [16384, 2048], P('sp', 'tp'), may hold values from -6 to 6
- floor_gap: float32 [2048], P('tp'), may hold values from 0 to 1, as said below
- head_gain: float32 [128], replicated, may hold values from 0.1 to 1.9
- stream: bfloat16 [16384, 2048], P('sp', 'tp'), may hold values from -40 to 40
- out_proj: bfloat16 [2048, 2048], P(None, 'tp'), may hold values from -0.125 to 0.125
- norm_gain: float32 [2048], P('tp'), may hold values from 0.1 to 1.9
- route_ids: int32 [16384, 2], P('sp'), may hold values from 0 to 31, all different within a row; in each aligned block of 512 rows (0 to 511, 512 to 1023, ...) at most 64 rows name the same one
- route_weights: float32 [16384, 2], P('sp'), may hold values from 0.1 to 1.5
- expert_gate: bfloat16 [32, 2048, 2048], P('sp', None, 'tp'), may hold values from -0.125 to 0.125
- expert_up: bfloat16 [32, 2048, 2048], P('sp', None, 'tp'), may hold values from -0.125 to 0.125
- expert_down: bfloat16 [32, 2048, 2048], P('sp', None, 'tp'), may hold values from -0.125 to 0.125
- shared_gate: bfloat16 [2048, 2048], P(None, 'tp'), may hold values from -0.125 to 0.125
- shared_up: bfloat16 [2048, 2048], P(None, 'tp'), may hold values from -0.125 to 0.125
- shared_down: bfloat16 [2048, 2048], P(None, 'tp'), may hold values from -0.125 to 0.125
Outputs:
- layer_out: bfloat16 [16384, 2048], P('sp', 'tp')
Inputs may be any that keep to these rules, and one draw needn't show every extreme that they name: `route_ids`: in each aligned block of 512 rows every expert is named by at most 64 rows, a bound that some block reaches; the 2 experts of a row differ. `floor_gap`: every entry is positive and at most 0.12.
All inputs are finite; a program needn't handle non-finite values.
Results may differ from a plain program's by a relative error of at most 0.008.
Values may be sent and summed in bfloat16 or wider, within the bound.
A program may use at most 64 MiB of HBM per device.

v0:
```python
import jax
import jax.numpy as jnp
from jax import lax
from jax.sharding import Mesh
from jax.sharding import PartitionSpec as P

D = 2048
HEAD = 128
SPAN = 64
TOP_K = 2
SP = ("sp_0", "sp_1")
TP = ("tp_0", "tp_1")


EPS = 1e-06


def neutral_like(value, identity):
    return jax.tree.map(
        lambda a, e: jnp.broadcast_to(jnp.asarray(e, a.dtype), a.shape), value, identity
    )


def gathered_once(value, axis):
    leaves = jax.tree.leaves(value)
    order = sorted(range(len(leaves)), key=lambda k: -leaves[k].size)
    width = (1, *leaves[order[0]].shape)[-1]
    lines = [
        jnp.pad(leaves[k].reshape(-1), (0, -leaves[k].size % width)).reshape(-1, width)
        for k in order
    ]
    both, at, found = (lax.all_gather(jnp.concatenate(lines), axis), 0, {})
    for k, line in zip(order, lines):
        slab = both[:, at : at + len(line)].reshape(len(both), -1)
        found[k] = slab[:, : leaves[k].size].reshape(-1, *leaves[k].shape)
        at += len(line)
    numbers = iter(range(len(leaves)))
    return jax.tree.map(lambda _: found[next(numbers)], value)


def prefix_by_axis(value, axes, combine, identity):
    before = start = neutral_like(value, identity)
    total = value
    for axis in reversed(axes):
        peers, mine = (lax.axis_size(axis), lax.axis_index(axis))
        pieces = gathered_once(total, axis)
        inside, total = (start, start)
        for k in range(peers):
            passed = k < mine
            total = combine(total, jax.tree.map(lambda part: part[k], pieces))
            inside = jax.tree.map(lambda new, old: jnp.where(passed, new, old), total, inside)
        before = combine(inside, before)
    return before


def sent_to_all(value, axis):
    copies = jnp.broadcast_to(value, (lax.axis_size(axis), *value.shape))
    return lax.all_to_all(copies, axis, split_axis=0, concat_axis=0, tiled=True)


def joined_along(pieces, dim):
    lengths = list(pieces.shape[1:])
    lengths[dim] *= pieces.shape[0]
    return jnp.moveaxis(pieces, 0, dim).reshape(lengths)


def gather_directly(value, axis, dim):
    pieces = sent_to_all(value, axis)
    return joined_along(pieces, dim)


def one_axis_at_a_time(value, axes):
    for axis in axes:
        value = lax.psum(value, axis)
    return value


def sent_together(arrays, axis, dim, along):
    widths = [a.shape[along] for a in arrays]
    both = jnp.concatenate(arrays, axis=along)
    filled = lax.all_gather(both, axis, axis=dim, tiled=True)
    return tuple(jnp.split(filled, [sum(widths[:k]) for k in range(1, len(widths))], axis=along))


def span_step(memory, blocks):
    queries, leakage, values, log_keep = blocks
    length = queries.shape[1]
    growth = jnp.cumsum(log_keep, axis=1)
    causal = jnp.tril(jnp.ones((length, length), dtype=bool))
    spread = growth[:, :, None, :] - growth[:, None, :, :]
    decays = jnp.exp(jnp.where(causal[None, :, :, None], spread, -jnp.inf))
    scores = jnp.einsum("htd,hsd,htsd->hts", queries, leakage, decays)
    within = jnp.einsum("hts,hsv->htv", scores, values)
    carried = jnp.einsum("htd,hdv->htv", queries * jnp.exp(growth), memory)
    closing = growth[:, -1:, :]
    memory = jnp.exp(closing[:, 0, :, None]) * memory + jnp.einsum(
        "hsd,hsv->hdv", leakage * jnp.exp(closing - growth), values
    )
    return (memory, within + carried)


def recurrence(queries, leakage, values, log_keep, memory):
    head_count, length, channels = queries.shape
    number = length // SPAN

    def blocked(array):
        return array.reshape(head_count, number, SPAN, channels).transpose(1, 0, 2, 3)

    memory, outputs = lax.scan(
        span_step, memory, (blocked(queries), blocked(leakage), blocked(values), blocked(log_keep))
    )
    return outputs.transpose(1, 0, 2, 3).reshape(head_count, length, channels)


def chain(earlier, later):
    return (earlier[0] * later[0], later[0][:, :, None] * earlier[1] + later[1])


def pad_rows(array):
    return jnp.concatenate([array, jnp.zeros((1, array.shape[1]), array.dtype)], axis=0)


def matmul(left, right):
    return jnp.dot(left, right, preferred_element_type=jnp.float32)


def body(
    query_pre,
    forget_pre,
    values_in,
    gate_pre,
    floor_gap,
    head_gain,
    stream,
    out_proj,
    norm_gain,
    route_ids,
    route_weights,
    expert_gate,
    expert_up,
    expert_down,
    shared_gate,
    shared_up,
    shared_down,
):
    length, local = query_pre.shape
    head_count = local // HEAD

    def split_heads(array):
        return array.astype(jnp.float32).reshape(length, head_count, HEAD).transpose(1, 0, 2)

    queries = jax.nn.silu(split_heads(query_pre))
    leakage = floor_gap.reshape(head_count, 1, HEAD) * jax.nn.sigmoid(-split_heads(forget_pre))
    log_keep = jnp.log1p(-leakage)
    values = split_heads(values_in)
    growth = jnp.cumsum(log_keep, axis=1)
    closing = growth[:, -1:, :]
    summary = jnp.einsum("hsd,hsv->hdv", leakage * jnp.exp(closing - growth), values)
    through = jnp.exp(closing[:, 0, :])
    unused, incoming = prefix_by_axis(
        (through, summary), SP, chain, (jnp.ones_like(through), jnp.zeros_like(summary))
    )
    outputs = recurrence(queries, leakage, values, log_keep, jnp.zeros_like(summary))
    outputs = outputs + jnp.einsum("htd,hdv->htv", queries * jnp.exp(growth), incoming)
    scaled = (
        outputs * lax.rsqrt(jnp.mean(outputs * outputs, axis=2, keepdims=True) + EPS) * head_gain
    )
    gated = scaled * jax.nn.silu(split_heads(gate_pre))
    mixed = gated.transpose(1, 0, 2).reshape(length, local).astype(jnp.bfloat16)
    projected = matmul(gather_directly(mixed, TP, 1), out_proj)
    residual = stream.astype(jnp.float32) + projected
    squares = one_axis_at_a_time(jnp.sum(residual * residual, axis=1), TP)
    normed = (residual * lax.rsqrt(squares / D + EPS)[:, None] * norm_gain).astype(jnp.bfloat16)
    experts = lax.axis_size(SP) * expert_gate.shape[0]
    capacity = 2 * TOP_K * length // experts
    flat_ids = route_ids.reshape(-1)
    matches = (flat_ids[:, None] == jnp.arange(experts, dtype=jnp.int32)[None, :]).astype(jnp.int32)
    earlier_hits = jnp.cumsum(matches, axis=0) - matches
    target = flat_ids * capacity + jnp.sum(earlier_hits * matches, axis=1)
    sender = (
        jnp.full((experts * capacity,), length, jnp.int32)
        .at[target]
        .set(jnp.arange(length * TOP_K, dtype=jnp.int32) // TOP_K)
    )
    gate_slice = expert_gate[0]
    up_slice = expert_up[0]
    down_slice = expert_down[0]
    arrived = lax.all_to_all(pad_rows(normed)[sender], SP, split_axis=0, concat_axis=0, tiled=True)
    own_rows, routed_rows = sent_together((normed, arrived), TP, 1, 0)
    shared_gate_part = matmul(own_rows, shared_gate)
    shared_up_part = matmul(own_rows, shared_up)
    routed_gate_part = matmul(routed_rows, gate_slice)
    routed_up_part = matmul(routed_rows, up_slice)
    shared_hidden = (jax.nn.silu(shared_gate_part) * shared_up_part).astype(jnp.bfloat16)
    routed_hidden = (jax.nn.silu(routed_gate_part) * routed_up_part).astype(jnp.bfloat16)
    full_shared, full_routed = (
        lax.all_gather(shared_hidden, TP, axis=1, tiled=True),
        lax.all_gather(routed_hidden, TP, axis=1, tiled=True),
    )
    shared_out = matmul(full_shared, shared_down)
    expert_result = matmul(full_routed, down_slice).astype(jnp.bfloat16)
    returned = lax.all_to_all(expert_result, SP, split_axis=0, concat_axis=0, tiled=True)
    picked = returned[target].astype(jnp.float32).reshape(length, TOP_K, returned.shape[1])
    routed = jnp.sum(picked * route_weights[:, :, None], axis=1)
    return (residual + shared_out + routed).astype(jnp.bfloat16)


def solution(mesh):
    finer = Mesh(mesh.devices.reshape(16, 2, 4, 4), ("sp_0", "sp_1", "tp_0", "tp_1"))
    in_specs = (
        P(SP, TP),
        P(SP, TP),
        P(SP, TP),
        P(SP, TP),
        P(TP),
        P(),
        P(SP, TP),
        P(None, TP),
        P(TP),
        P(SP, None),
        P(SP, None),
        P(SP, None, TP),
        P(SP, None, TP),
        P(SP, None, TP),
        P(None, TP),
        P(None, TP),
        P(None, TP),
    )
    out_specs = P(SP, TP)
    return jax.shard_map(body, mesh=finer, in_specs=in_specs, out_specs=out_specs, check_vma=False)
```

profile of v0, /device:TPU:2, one launch (start us, length us, event | category | flops | bytes accessed | tf_op | source)
XLA Modules:
  0.0 454.3 jit_solution(16247520927167944288)
XLA Ops:
  13.5 24.4 %while.13 = (s32[]{:T(128)}, f32[1,128,128]{2,1,0:T(8,128)S(1)}, f32[8,1,64,128]{3,2,1,0:T(8,128)S(1)}, f32[8,1,64,128]{3,2,1,0:T(8,128)S(1)}, f32[8,1,64,128]{3...) while((s32[]{:T(128)}, f32[1,128,128]{2,1,0:T(8,128)S(1)}, ...), condition=%wide.region_2.3_spmd.clone, body=%wide.region_0.0_spmd.clone.sunk | while | flops 8478723 | bytes 5051520 | solution.py:109
  38.2 50.0 %all-gather.15.cloned.1.call-done = f32[16,129,128]{2,1,0:T(8,128)} async-done(((f32[1,129,128]{2,1,0:T(8,128)}), f32[16,129,128]{2,1,0:T(8,128)}) %all-gather.15.cloned.1.call-update) | async-done | bytes 1056784 | tf_op jit(solution)/shard_map/all_gather | solution.py:32
  89.0 1.9 multiply_reduce_fusion.1
  92.6 7.4 %all-to-all-start = ((bf16[16,512,128]{1,2,0:T(8,128)(2,1)}), bf16[16,512,128]{1,2,0:T(8,128)(2,1)S(1)}, u32[]{:S(2)}, u32[]{:S(2)}) async-start(bf16[16,512,128]{1,2,0:T(8,128)(2,1)} %broadcast_in_dim.48), calls=%async_computation | async-start | bytes 4194304 | tf_op jit(solution)/shard_map/all_to_all | solution.py:58
  100.6 9.0 %reduce-window.16 = s32[32,8,128]{2,1,0:T(8,128)S(1)} reduce-window(s32[32,8,128]{2,1,0:T(8,128)S(1)} %fusion.72, s32[]{:T(128)} %constant.41.clone.1), window={size=1x1x128 pad=0_0x0_0x127_0}, to_apply=%region_9.10 | reduce-window | flops 4161536 | bytes 262148 | tf_op jit(solution)/shard_map/reduce-window.2
  110.5 4.3 scatter_custom_fusion
  114.8 3.6 all-to-all-done
  120.3 11.1 %psum.14 = f32[512]{0:T(512)S(1)} all-reduce(f32[512]{0:T(512)S(1)} %get-tuple-element.138), channel_id=1, replica_groups=mesh['sp_0'=16,'sp_1'=2,'tp_0'=4,'tp_1'=4] {'tp_0'}, use_global_device_ids=true, to_apply=%region_7.8 | all-reduce | flops 512 | bytes 4096 | tf_op jit(solution)/shard_map/psum | solution.py:74
  131.4 9.5 %psum.15 = f32[512]{0:T(512)S(1)} all-reduce(f32[512]{0:T(512)S(1)} %psum.14), channel_id=1, replica_groups=mesh['sp_0'=16,'sp_1'=2,'tp_0'=4,'tp_1'=4] {'tp_1'}, use_global_device_ids=true, to_apply=%region_8.9 | all-reduce | flops 512 | bytes 4096 | tf_op jit(solution)/shard_map/psum | solution.py:74
  141.1 6.2 %gather_fusion = bf16[2048,128]{1,0:T(8,128)(2,1)S(1)} fusion(bf16[513,128]{1,0:T(8,128)(2,1)S(1)} %concatenate.14, s32[2048]{0:T(1024)S(1)} %fusion.147), kind=kCustom, calls=%fused_computation | custom fusion | bytes 1056768 | tf_op jit(solution)/shard_map/gather | solution.py:188
  147.3 41.7 %all_to_all.29 = bf16[32,64,128]{2,1,0:T(8,128)(2,1)S(1)} all-to-all(bf16[32,64,128]{2,1,0:T(8,128)(2,1)S(1)} %bitcast.243), channel_id=1, replica_groups=mesh['sp_0'=16,'sp_1'=2,'tp_0'=4,'tp_1'=4] {'sp_0','sp_1'}, dimensions={0} | all-to-all | bytes 1048576 | tf_op jit(solution)/shard_map/all_to_all | solution.py:188
  190.1 90.3 %all-gather.9.cloned.1.call-done = bf16[2560,2048]{1,0:T(8,128)(2,1)} async-done(((bf16[2560,128]{1,0:T(8,128)(2,1)}), bf16[2560,2048]{1,0:T(8,128)(2,1)}) %all-gather.9.cloned.1.call-update) | async-done | bytes 10485776 | tf_op jit(solution)/shard_map/all_gather | solution.py:81
  280.4 5.9 %fusion.30 = f32[2048,128]{1,0:T(8,128)S(1)} fusion(bf16[2560,2048]{1,0:T(8,128)(2,1)} %all-gather.9.cloned.1.call-done, bf16[1,2048,128]{2,1,0:T(8,128)(2,1)S(1)} %copy-done), kind=kOutput, calls=%fused_computation.42 | convolution fusion | flops 1073741824 | bytes 9961472 | tf_op jit(solution)/shard_map/dot_general | solution.py:124
  286.8 3.2 fusion.35
  290.1 2.5 fusion.40
  292.6 3.1 fusion.47
  295.8 86.4 %all-gather.13.cloned.1.call-done = bf16[2048,2048]{1,0:T(8,128)(2,1)} async-done(((bf16[2048,128]{1,0:T(8,128)(2,1)}), bf16[2048,2048]{1,0:T(8,128)(2,1)}) %all-gather.13.cloned.1.call-update) | async-done | bytes 8388624 | tf_op jit(solution)/shard_map/all_gather | solution.py:198
  382.2 6.5 %convolution_convert_fusion = bf16[2048,128]{1,0:T(8,128)(2,1)} fusion(bf16[2048,2048]{1,0:T(8,128)(2,1)} %all-gather.13.cloned.1.call-done, bf16[1,2048,128]{2,1,0:T(8,128)(2,1)S(1)} %copy-done.15), kind=kOutput, calls=%fused_computation.45 | convolution fusion | flops 1074003968 | bytes 9437184 | tf_op jit(solution)/shard_map/dot_general | solution.py:124
  388.7 12.7 %all-to-all-start.2 = ((bf16[32,64,128]{2,1,0:T(8,128)(2,1)}), bf16[32,64,128]{2,1,0:T(8,128)(2,1)S(1)}, u32[]{:S(2)}, u32[]{:S(2)}) async-start(bf16[32,64,128]{2,1,0:T(8,128)(2,1)} %bitcast.52), calls=%async_computation.2 | async-start | bytes 1048576 | tf_op jit(solution)/shard_map/all_to_all | solution.py:202
  401.6 33.6 %all-to-all-done.2 = bf16[32,64,128]{2,1,0:T(8,128)(2,1)S(1)} async-done(((bf16[32,64,128]{2,1,0:T(8,128)(2,1)}), bf16[32,64,128]{2,1,0:T(8,128)(2,1)S(1)}, u32[]{:S(2)}, u32[]{:S(2)}) %all-to-all-start.2) | async-done | bytes 524320 | tf_op jit(solution)/shard_map/all_to_all | solution.py:202
  435.2 3.2 gather_fusion.1
  438.4 2.8 fusion.50
  441.3 3.5 all-gather.11.cloned.1.call-done
  444.8 3.0 fusion.46
  (187 shorter events, 38.6 us)
Async XLA Ops:
  6.5 273.9 %copy-start = (bf16[1,2048,128]{2,1,0:T(8,128)(2,1)S(1)}, bf16[1,2048,128]{2,1,0:T(8,128)(2,1)}, u32[]{:S(2)}) copy-start(bf16[1,2048,128]{2,1,0:T(8,128)(2,1)} %param.30) | copy-start | bytes 1572868
  6.5 81.7 %all-gather.15.cloned.1.call-start = ((), (), s32[]{:S(2)}) async-start(), calls=%async_computation.6 | async-start | bytes 1183744 | tf_op jit(solution)/shard_map/all_gather | solution.py:32
  8.4 1.4 copy-start.2
  8.5 1.4 copy-start.8
  9.6 3.5 copy-start.4
  13.5 24.6 %copy-start.5 = (bf16[512,128]{1,0:T(8,128)(2,1)S(1)}, bf16[512,128]{1,0:T(8,128)(2,1)}, u32[]{:S(2)}) copy-start(bf16[512,128]{1,0:T(8,128)(2,1)} %param.22) | copy-start | bytes 393220
  37.9 53.0 %copy-start.9 = (f32[128]{0:T(128)S(1)}, f32[128]{0:T(128)}, u32[]{:S(2)}) copy-start(f32[128]{0:T(128)} %param.24) | copy-start | bytes 1540
  92.6 7.5 %copy-start.6 = (s32[512,2]{0,1:T(2,128)S(1)}, s32[512,2]{0,1:T(2,128)}, u32[]{:S(2)}) copy-start(s32[512,2]{0,1:T(2,128)} %param.28) | copy-start | bytes 12292
  92.6 25.8 %all-to-all-start = ((bf16[16,512,128]{1,2,0:T(8,128)(2,1)}), bf16[16,512,128]{1,2,0:T(8,128)(2,1)S(1)}, u32[]{:S(2)}, u32[]{:S(2)}) async-start(bf16[16,512,128]{1,2,0:T(8,128)(2,1)} %broadcast_in_dim.48), calls=%async_computation | async-start | bytes 4194304 | tf_op jit(solution)/shard_map/all_to_all | solution.py:58
  100.0 18.4 %copy-start.3 = (bf16[512,128]{1,0:T(8,128)(2,1)S(1)}, bf16[512,128]{1,0:T(8,128)(2,1)}, u32[]{:S(2)}) copy-start(bf16[512,128]{1,0:T(8,128)(2,1)} %param.25) | copy-start | bytes 393220
  100.0 180.4 %all-gather.9.cloned.1.call-start = ((), (), s32[]{:S(2)}) async-start(), calls=%async_computation.3 | async-start | bytes 11141120 | tf_op jit(solution)/shard_map/all_gather | solution.py:81
  109.7 31.2 %copy-start.10 = (f32[128]{0:T(128)S(1)}, f32[128]{0:T(128)}, u32[]{:S(2)}) copy-start(f32[128]{0:T(128)} %param.27) | copy-start | bytes 1540
  189.9 96.5 %copy-start.12 = (bf16[1,2048,128]{2,1,0:T(8,128)(2,1)S(1)}, bf16[1,2048,128]{2,1,0:T(8,128)(2,1)}, u32[]{:S(2)}) copy-start(bf16[1,2048,128]{2,1,0:T(8,128)(2,1)} %param.31) | copy-start | bytes 1572868
  189.9 192.3 %all-gather.13.cloned.1.call-start = ((), (), s32[]{:S(2)}) async-start(), calls=%async_computation.5 | async-start | bytes 8912896 | tf_op jit(solution)/shard_map/all_gather | solution.py:198
  280.4 6.4 %copy-start.11 = (bf16[2560,2048]{1,0:T(8,128)(2,1)S(1)}, bf16[2560,2048]{1,0:T(8,128)(2,1)}, u32[]{:S(2)}) copy-start(bf16[2560,2048]{1,0:T(8,128)(2,1)} %all-gather.9.cloned.1.call-done) | copy-start | bytes 31457284
  286.8 3.3 copy-start.13
  290.0 2.6 copy-start.14
  290.1 154.7 %all-gather.11.cloned.1.call-start = ((), (), s32[]{:S(2)}) async-start(), calls=%async_computation.4 | async-start | bytes 2228224 | tf_op jit(solution)/shard_map/all_gather | solution.py:197
  292.6 89.6 %copy-start.15 = (bf16[1,2048,128]{2,1,0:T(8,128)(2,1)S(1)}, bf16[1,2048,128]{2,1,0:T(8,128)(2,1)}, u32[]{:S(2)}) copy-start(bf16[1,2048,128]{2,1,0:T(8,128)(2,1)} %param.32) | copy-start | bytes 1572868
  295.8 105.7 %copy-start.7 = (f32[512,2]{0,1:T(2,128)S(1)}, f32[512,2]{0,1:T(2,128)}, u32[]{:S(2)}) copy-start(f32[512,2]{0,1:T(2,128)} %param.29) | copy-start | bytes 12292
  388.7 56.0 %copy-start.1 = (bf16[2048,128]{1,0:T(8,128)(2,1)S(1)}, bf16[2048,128]{1,0:T(8,128)(2,1)}, u32[]{:S(2)}) copy-start(bf16[2048,128]{1,0:T(8,128)(2,1)} %param.35) | copy-start | bytes 1572868
  388.7 46.5 %all-to-all-start.2 = ((bf16[32,64,128]{2,1,0:T(8,128)(2,1)}), bf16[32,64,128]{2,1,0:T(8,128)(2,1)S(1)}, u32[]{:S(2)}, u32[]{:S(2)}) async-start(bf16[32,64,128]{2,1,0:T(8,128)(2,1)} %bitcast.52), calls=%async_computation.2 | async-start | bytes 1048576 | tf_op jit(solution)/shard_map/all_to_all | solution.py:202
Sparse Core Ops, SparseCore 0:
  13.0 75.1 all-gather.14
  190.0 90.3 all-gather.8
  290.2 91.9 all-gather.12
  385.1 59.6 all-gather.10
where the time goes:
time: 455 us; the launch traced here: 454 us
  waiting for transfers between devices  267 us (59%)
  blocking collectives  64.2 us (14%)
  other arithmetic  35.4 us (8%)
  matrix products  32.5 us (7%)
  starting transfers between devices  20.4 us (4%)
  local copies, waits for them, and re-layouts  20.2 us (4%)
  between operations  13.7 us (3%)
    all_gather x1, waiting for transfers between devices, sent_together(): filled = lax.all_gather(both, axis, axis=dim, tiled=True)  90.3 us
    all_gather x1, waiting for transfers between devices, body(): lax.all_gather(routed_hidden, TP, axis=1, tiled=True)  86.4 us
    all_gather x1, waiting for transfers between devices, gathered_once(): both, at, found = (lax.all_gather(jnp.concatenate(lines), axis), 0, {})  50 us
    all_to_all x1, blocking collectives, body(): lax.all_to_all(pad_rows(normed)[sender], SP, split_axis=0, concat_axis=0,...  41.7 us
    all_to_all x1, waiting for transfers between devices, body(): lax.all_to_all(expert_result, SP, split_axis=0, concat_axis=0, tiled=True)  33.6 us
    dot_general x7, matrix products, matmul(): return jnp.dot(left, right, preferred_element_type=jnp.float32)  26.2 us
    psum x2, blocking collectives, one_axis_at_a_time(): value = lax.psum(value, axis)  20.6 us
    dot_general x8, other arithmetic, span_step(): scores = jnp.einsum('htd,hsd,htsd->hts', queries, leakage, decays)  13.8 us
  transfers between devices with their start and end apart: 6, of which 6 were waited for; matrix products, arithmetic and copies ran while one was open for 13% of the time, Pallas kernels for 0%

commit v1 on v0

v1 whole, which is shorter than its diff:
```python
import functools

import jax
import jax.numpy as jnp
from jax import lax
from jax.experimental import pallas as pl
from jax.experimental.pallas import tpu as pltpu
from jax.sharding import Mesh
from jax.sharding import PartitionSpec as P

D = 2048
T = 512
W = 128
CAP = 64
EPS = 1e-06
MESH = pl.DeviceIdType.MESH
F32 = jnp.float32
BF16 = jnp.bfloat16


class Sems:
    def __init__(self):
        self.used = 0

    def take(self, count):
        first = self.used
        self.used += count
        return first


SEM = Sems()
LOCAL_W = SEM.take(7)
GATHER_W = [(SEM.take(3), SEM.take(3)) for _ in range(3)]
PAIR = SEM.take(2)
PAIR_H = SEM.take(2)
STATE_S, STATE_R = SEM.take(16), SEM.take(16)
DECAY_S, DECAY_R = SEM.take(16), SEM.take(16)
SQUARE_S, SQUARE_R = SEM.take(16), SEM.take(16)
OUT_S, OUT_R = SEM.take(32), SEM.take(32)
BACK_S, BACK_R = SEM.take(32), SEM.take(32)
ALONG_A = [(SEM.take(3), SEM.take(3)) for _ in range(5)]
ALONG_B = [[SEM.take(4) for _ in range(8)] for _ in range(5)]


def dot(left, right):
    return jnp.dot(left, right, preferred_element_type=F32)


def dot_last(left, right):
    return lax.dot_general(left, right, (((1,), (1,)), ((), ())), preferred_element_type=F32)


def dot_first(left, right):
    return lax.dot_general(left, right, (((0,), (0,)), ((), ())), preferred_element_type=F32)


def silu(v):
    return v * jax.nn.sigmoid(v)


def in_three(value):
    high = value.astype(BF16)
    rest = value - high.astype(F32)
    middle = rest.astype(BF16)
    low = (rest - middle.astype(F32)).astype(BF16)
    return high, middle, low


def diagonal():
    return lax.broadcasted_iota(jnp.int32, (W, W), 0) == lax.broadcasted_iota(jnp.int32, (W, W), 1)


def to_column(row):
    eye = diagonal()
    return jnp.concatenate(
        [
            jnp.sum(jnp.where(eye, row[:, k * W : (k + 1) * W], 0.0), axis=1, keepdims=True)
            for k in range(row.shape[1] // W)
        ],
        axis=0,
    )


def to_row(column):
    eye = diagonal()
    return jnp.concatenate(
        [
            jnp.sum(jnp.where(eye, column[k * W : (k + 1) * W], 0.0), axis=0, keepdims=True)
            for k in range(column.shape[0] // W)
        ],
        axis=1,
    )


def kernel(
    zs,
    query_ref,
    forget_ref,
    value_ref,
    gatep_ref,
    gap_ref,
    head_gain_ref,
    stream_ref,
    norm_gain_ref,
    ids_ref,
    weights_ref,
    proj_hbm,
    sg_hbm,
    su_hbm,
    sd_hbm,
    eg_hbm,
    eu_hbm,
    ed_hbm,
    out_ref,
    wo,
    wsg,
    wsu,
    wsd,
    weg,
    weu,
    wed,
    pair_mine,
    pair_other,
    state_send,
    state_recv,
    decay_send,
    decay_recv,
    half_mine,
    half_other,
    squares,
    x_mixed,
    x_normed,
    x_shared,
    x_rows,
    x_hidden,
    send_rows,
    recv_rows,
    result,
    gathered,
    back,
    choose,
    pick0,
    pick1,
    residual,
    shared_out,
    within,
    carried,
    gate_act,
    slots,
    sems,
):
    z, c = lax.axis_index("z"), lax.axis_index("c")
    y, x = lax.axis_index("y"), lax.axis_index("x")
    me = z * 2 + c
    spn = zs * 2
    j = y * 4 + x
    a = x * (1 - c) + y * c
    b = y * (1 - c) + x * c
    group = spn * CAP // 4

    def plane(a_to, b_to):
        return (z, c, b_to * (1 - c) + a_to * c, a_to * (1 - c) + b_to * c)

    def number(a_to, b_to):
        return (b_to * (1 - c) + a_to * c) * 4 + a_to * (1 - c) + b_to * c

    def column(number_of):
        return pl.ds(pl.multiple_of(number_of * W, W), W)

    def rows_of(number_of, count):
        return pl.ds(pl.multiple_of(number_of * count, count), count)

    def remote(src, dst, sent, received, where):
        return pltpu.make_async_remote_copy(
            src_ref=src,
            dst_ref=dst,
            send_sem=sems.at[sent],
            recv_sem=sems.at[received],
            device_id=where,
            device_id_type=MESH,
        )

    barrier = pltpu.get_barrier_semaphore()

    def greet_column(i, carry):
        to = (me + i) % spn
        pl.semaphore_signal(barrier, inc=1, device_id=(to // 2, to % 2, y, x), device_id_type=MESH)
        return carry

    def greet_plane(i, carry):
        to = (j + i) % 16
        pl.semaphore_signal(barrier, inc=1, device_id=(z, c, to // 4, to % 4), device_id_type=MESH)
        return carry

    lax.fori_loop(1, spn, greet_column, 0)
    lax.fori_loop(1, 16, greet_plane, 0)

    local = [
        pltpu.make_async_copy(src, dst, sems.at[LOCAL_W + k])
        for k, (src, dst) in enumerate(
            [
                (eg_hbm, weg.at[:, column(a)]),
                (proj_hbm, wo),
                (sg_hbm, wsg),
                (su_hbm, wsu),
                (sd_hbm, wsd),
                (eu_hbm, weu.at[:, column(a)]),
                (ed_hbm, wed.at[:, column(a)]),
            ]
        )
    ]
    for copy in local:
        copy.start()

    leakage = gap_ref[...] * jax.nn.sigmoid(-forget_ref[...].astype(F32))
    log_keep = jnp.log1p(-leakage)
    lower = (
        lax.broadcasted_iota(jnp.int32, (T, T), 0) >= lax.broadcasted_iota(jnp.int32, (T, T), 1)
    ).astype(BF16)
    high, middle, low = in_three(log_keep)
    growth = dot(lower, high) + dot(lower, middle) + dot(lower, low)
    closing = growth[T - 1 : T, :]
    values = value_ref[...]
    state = dot_first(values, (leakage * jnp.exp(closing - growth)).astype(BF16))
    through = jnp.exp(closing)
    pair_mine[0:W, :] = state
    pair_mine[W : W + 8, :] = jnp.broadcast_to(through, (8, W))

    pl.semaphore_wait(barrier, spn - 1 + 15)

    swap = remote(pair_mine, pair_other, PAIR, PAIR + 1, (z, 1 - c, y, x))
    swap.start()

    def gather_weights(which, src, dst):
        sent, received = GATHER_W[which]
        copies = []
        for i in (1, 3, 2):
            copies.append(
                remote(src, dst.at[:, column(a)], sent + i - 1, received + i - 1, plane((a + i) % 4, b))
            )
        for copy in copies:
            copy.start()

        def finish():
            local[{0: 0, 1: 5, 2: 6}[which]].wait()
            for i in (1, 3, 2):
                from_a = (a + 4 - i) % 4
                remote(
                    src, dst.at[:, column(from_a)], sent + i - 1, received + i - 1, plane(from_a, b)
                ).wait_recv()

        return copies, finish

    gate_copies, gate_ready = gather_weights(0, eg_hbm, weg)

    swap.wait_recv()
    other_state, other_through = pair_other[0:W, :], pair_other[W : W + 1, :]
    mine_first = c == 0
    first = jnp.where(mine_first, state, other_state)
    second = jnp.where(mine_first, other_state, state)
    second_through = jnp.where(mine_first, other_through, through)
    total = first * second_through + second
    state_send[...] = jnp.where(mine_first, total[0:CAP, :], total[CAP:W, :]).astype(BF16)
    decay_send[...] = through * other_through

    def state_copy(to, slot):
        return remote(state_send, state_recv.at[slot], STATE_S + to, STATE_R + slot, (to, c, y, x))

    def decay_copy(to, slot):
        return remote(decay_send, decay_recv.at[slot], DECAY_S + to, DECAY_R + slot, (to, c, y, x))

    def send_state(i, carry):
        to = zs - 1 - i
        state_copy(to, z).start()
        decay_copy(to, z).start()
        return carry

    lax.fori_loop(0, zs - 1 - z, send_state, 0)

    queries = silu(query_ref[...].astype(F32))
    centre = growth[T // 2 - 1 : T // 2, :]
    scaled_q = (queries * jnp.exp(growth - centre)).astype(BF16)
    scaled_k = (leakage * jnp.exp(centre - growth)).astype(BF16)
    carried[...] = (queries * jnp.exp(growth)).astype(BF16)
    gate_act[...] = silu(gatep_ref[...].astype(F32)) * head_gain_ref[...]
    for k in range(T // W):
        upto = (k + 1) * W
        scores = dot_last(scaled_q[k * W : upto, :], scaled_k[0:upto, :])
        causal = lax.broadcasted_iota(jnp.int32, (W, upto), 0) + k * W >= lax.broadcasted_iota(
            jnp.int32, (W, upto), 1
        )
        scores = jnp.where(causal, scores, 0.0).astype(BF16)
        within[k * W : upto, :] = dot(scores, values[0:upto, :])

    ids = ids_ref[...]
    lanes = lax.broadcasted_iota(jnp.int32, (W, T), 0)
    hits0, hits1 = lanes == ids[0:1, :], lanes == ids[1:2, :]
    before = (
        lax.broadcasted_iota(jnp.int32, (T, T), 0) < lax.broadcasted_iota(jnp.int32, (T, T), 1)
    ).astype(BF16)
    earlier = dot((hits0 | hits1).astype(BF16), before)
    place = earlier + lanes.astype(F32) * CAP
    slot0 = jnp.sum(jnp.where(hits0, place, 0.0), axis=0, keepdims=True)
    slot1 = jnp.sum(jnp.where(hits1, place, 0.0), axis=0, keepdims=True)
    slots[0] = jnp.broadcast_to(to_column(slot0), (T, W))
    slots[1] = jnp.broadcast_to(to_column(slot1), (T, W))

    def build(i, carry):
        base = (i * W).astype(F32)
        down = lax.broadcasted_iota(jnp.int32, (W, T), 0).astype(F32) + base
        choose[rows_of(i, W), :] = ((down == slot0) | (down == slot1)).astype(BF16)
        along = lax.broadcasted_iota(jnp.int32, (T, W), 1).astype(F32) + base
        pick0[:, column(i)] = (slots[0] == along).astype(BF16)
        pick1[:, column(i)] = (slots[1] == along).astype(BF16)
        return carry

    lax.fori_loop(0, spn * CAP // W, build, 0)

    def take_state(k, held):
        state_copy(k, k).wait_recv()
        decay_copy(k, k).wait_recv()
        return held * decay_recv[k] + state_recv[k].astype(F32)

    half = lax.fori_loop(0, z, take_state, jnp.zeros((CAP, W), F32))
    half_mine[...] = half
    swap_half = remote(half_mine, half_other, PAIR_H, PAIR_H + 1, (z, 1 - c, y, x))
    swap_half.start()
    swap_half.wait_recv()
    theirs = half_other[...]
    incoming = jnp.concatenate(
        [jnp.where(mine_first, half, theirs), jnp.where(mine_first, theirs, half)], axis=0
    )
    incoming = jnp.where(
        mine_first, incoming, incoming * pair_other[W : W + 1, :] + pair_other[0:W, :]
    )
    outputs = within[...] + dot_last(carried[...], incoming.astype(BF16))
    mean = jnp.mean(outputs * outputs, axis=1, keepdims=True)
    x_mixed[:, column(j)] = (outputs * lax.rsqrt(mean + EPS) * gate_act[...]).astype(BF16)

    def gather_along_b(buffer, which, order, ready):
        sems_of = ALONG_B[which]
        rows = buffer.shape[0]
        upper, lower_half = pl.ds(0, rows // 2), pl.ds(rows // 2, rows // 2)
        every = pl.ds(0, rows)
        right, left = (b + 1) % 4, (b + 3) % 4
        sends = []

        def step(i, part, b_of, to, kind):
            block = buffer.at[part, column(number((a + 4 - i) % 4, b_of))]
            return remote(block, block, sems_of[2 * kind] + i, sems_of[2 * kind + 1] + i, plane(a, to))

        def start(copy):
            copy.start()
            sends.append(copy)

        def forward(i):
            step(i, every, left, right, 0).wait_recv()
            start(step(i, upper, left, right, 2))
            step(i, every, right, left, 1).wait_recv()
            start(step(i, lower_half, right, left, 3))

        last = None
        for i in order:
            ready(i)
            start(step(i, every, b, right, 0))
            start(step(i, every, b, left, 1))
            if last is not None:
                forward(last)
            last = i
        forward(last)

        def finish():
            opposite = (b + 2) % 4
            for i in order:
                step(i, upper, opposite, right, 2).wait_recv()
                step(i, lower_half, opposite, left, 3).wait_recv()
            return sends

        return finish

    def send_along_a(which, source_of, buffer):
        sent, received = ALONG_A[which]
        copies = []
        for i in (1, 3, 2):
            to = (a + i) % 4
            copies.append(
                remote(source_of(to), buffer.at[:, column(j)], sent + i - 1, received + i - 1, plane(to, b))
            )
            copies[-1].start()

        def ready(i):
            if i:
                from_a = (a + 4 - i) % 4
                block = buffer.at[:, column(number(from_a, b))]
                remote(block, block, sent + i - 1, received + i - 1, plane(from_a, b)).wait_recv()

        return copies, ready

    def gather_plane(buffer, which):
        own = buffer.at[:, column(j)]
        copies, ready = send_along_a(which, lambda to: own, buffer)
        finish = gather_along_b(buffer, which, (0, 1, 3, 2), ready)
        return lambda: copies + finish()

    pending = list(gate_copies)
    finish = gather_plane(x_mixed, 0)
    pending += finish()
    up_copies, up_ready = gather_weights(1, eu_hbm, weu)
    pending += up_copies

    local[1].wait()
    res = stream_ref[...].astype(F32) + dot(x_mixed[...], wo[...])
    residual[...] = res
    squares[j] = to_row(jnp.sum(res * res, axis=1, keepdims=True))

    def square_copy(to, slot):
        return remote(
            squares.at[slot], squares.at[slot], SQUARE_S + to, SQUARE_R + slot, (z, c, to // 4, to % 4)
        )

    def send_squares(i, carry):
        square_copy((j + i) % 16, j).start()
        return carry

    def wait_squares(i, carry):
        square_copy((j + i) % 16, (j + i) % 16).wait_recv()
        return carry

    lax.fori_loop(1, 16, send_squares, 0)
    lax.fori_loop(1, 16, wait_squares, 0)
    summed = jnp.sum(squares[...], axis=0)
    scale = to_column(lax.rsqrt(summed / D + EPS))
    normed = (res * scale * norm_gain_ref[...]).astype(BF16)
    x_normed[:, column(j)] = normed

    for k in range(spn * CAP // T):
        send_rows[k * T : (k + 1) * T, :] = dot(choose[k * T : (k + 1) * T, :], normed).astype(BF16)

    def out_copy(to, slot):
        return remote(
            send_rows.at[rows_of(to, CAP), :],
            recv_rows.at[rows_of(slot, CAP), :],
            OUT_S + to,
            OUT_R + slot,
            (to // 2, to % 2, y, x),
        )

    def send_out(i, carry):
        out_copy((me + i) % spn, me).start()
        return carry

    def wait_out(i, carry):
        out_copy((me + i) % spn, (me + i) % spn).wait_recv()
        return carry

    lax.fori_loop(1, spn, send_out, 0)
    recv_rows[rows_of(me, CAP), :] = send_rows[rows_of(me, CAP), :]

    finish = gather_plane(x_normed, 1)
    pending += finish()
    local[2].wait()
    local[3].wait()
    hidden = silu(dot(x_normed[...], wsg[...])) * dot(x_normed[...], wsu[...])
    x_shared[:, column(j)] = hidden.astype(BF16)
    finish = gather_plane(x_shared, 2)
    down_copies, down_ready = gather_weights(2, ed_hbm, wed)
    pending += down_copies
    pending += finish()
    local[4].wait()
    shared_out[...] = residual[...] + dot(x_shared[...], wsd[...])

    lax.fori_loop(1, spn, wait_out, 0)
    own_rows = pl.ds(pl.multiple_of(a * group, group), group)
    x_rows[:, column(j)] = recv_rows[own_rows, :]
    copies, ready = send_along_a(3, lambda to: recv_rows.at[rows_of(to, group), :], x_rows)
    pending += copies
    pending += gather_along_b(x_rows, 3, (0, 1, 3, 2), ready)()
    gate_ready()
    up_ready()
    for k in range(4):
        part = slice(k * (group // 4), (k + 1) * (group // 4))
        rows_in = x_rows[part, :]
        hidden = (silu(dot(rows_in, weg[...])) * dot(rows_in, weu[...])).astype(BF16)
        for n in range(4):
            x_hidden[part, column(number(n, b))] = hidden[:, n * W : (n + 1) * W]
    pending += gather_along_b(x_hidden, 4, (0, 1, 2, 3), lambda i: None)()
    down_ready()
    for k in range(4):
        part = slice(k * (group // 4), (k + 1) * (group // 4))
        rows_out = dot(x_hidden[part, :], wed[...]).astype(BF16)
        for n in range(4):
            result[n, part, :] = rows_out[:, n * W : (n + 1) * W]

    sent, received = ALONG_A[4]
    for i in (1, 3, 2):
        to = (a + i) % 4
        copy = remote(
            result.at[to], gathered.at[own_rows, :], sent + i - 1, received + i - 1, plane(to, b)
        )
        copy.start()
        pending.append(copy)
    gathered[own_rows, :] = result[a]
    for i in (1, 3, 2):
        from_a = (a + 4 - i) % 4
        remote(
            result.at[a], gathered.at[rows_of(from_a, group), :], sent + i - 1, received + i - 1, plane(from_a, b)
        ).wait_recv()

    def back_copy(to, slot):
        return remote(
            gathered.at[rows_of(to, CAP), :],
            back.at[rows_of(slot, CAP), :],
            BACK_S + to,
            BACK_R + slot,
            (to // 2, to % 2, y, x),
        )

    def send_back(i, carry):
        back_copy((me + i) % spn, me).start()
        return carry

    def wait_back(i, carry):
        back_copy((me + i) % spn, (me + i) % spn).wait_recv()
        return carry

    lax.fori_loop(1, spn, send_back, 0)
    back[rows_of(me, CAP), :] = gathered[rows_of(me, CAP), :]
    lax.fori_loop(1, spn, wait_back, 0)

    returned = back[...]
    weights = weights_ref[...]
    routed = dot(pick0[...], returned) * to_column(weights[0:1, :])
    routed += dot(pick1[...], returned) * to_column(weights[1:2, :])
    out_ref[...] = (shared_out[...] + routed).astype(BF16)

    swap.wait_send()
    swap_half.wait_send()
    for copy in pending:
        copy.wait_send()

    def drain_state(i, carry):
        state_copy(zs - 1 - i, z).wait_send()
        decay_copy(zs - 1 - i, z).wait_send()
        return carry

    def drain_squares(i, carry):
        square_copy((j + i) % 16, j).wait_send()
        return carry

    def drain_rows(i, carry):
        out_copy((me + i) % spn, me).wait_send()
        back_copy((me + i) % spn, me).wait_send()
        return carry

    lax.fori_loop(0, zs - 1 - z, drain_state, 0)
    lax.fori_loop(1, 16, drain_squares, 0)
    lax.fori_loop(1, spn, drain_rows, 0)


def layer(zs, *args):
    (
        query_pre,
        forget_pre,
        values_in,
        gate_pre,
        floor_gap,
        head_gain,
        stream,
        out_proj,
        norm_gain,
        route_ids,
        route_weights,
        expert_gate,
        expert_up,
        expert_down,
        shared_gate,
        shared_up,
        shared_down,
    ) = args
    rows = zs * 2 * CAP
    group = rows // 4
    vmem = pl.BlockSpec(memory_space=pltpu.VMEM)
    hbm = pl.BlockSpec(memory_space=pl.ANY)
    scratch = [
        *[pltpu.VMEM((D, W), BF16)] * 4,
        *[pltpu.VMEM((D, 4 * W), BF16)] * 3,
        *[pltpu.VMEM((W + 8, W), F32)] * 2,
        pltpu.VMEM((CAP, W), BF16),
        pltpu.VMEM((zs, CAP, W), BF16),
        pltpu.VMEM((1, W), F32),
        pltpu.VMEM((zs, 1, W), F32),
        *[pltpu.VMEM((CAP, W), F32)] * 2,
        pltpu.VMEM((16, 1, T), F32),
        *[pltpu.VMEM((T, D), BF16)] * 3,
        *[pltpu.VMEM((group, D), BF16)] * 2,
        *[pltpu.VMEM((rows, W), BF16)] * 2,
        pltpu.VMEM((4, group, W), BF16),
        *[pltpu.VMEM((rows, W), BF16)] * 2,
        pltpu.VMEM((rows, T), BF16),
        *[pltpu.VMEM((T, rows), BF16)] * 2,
        *[pltpu.VMEM((T, W), F32)] * 3,
        pltpu.VMEM((T, W), BF16),
        pltpu.VMEM((T, W), F32),
        pltpu.VMEM((2, T, W), F32),
        pltpu.SemaphoreType.DMA((SEM.used,)),
    ]
    return pl.pallas_call(
        functools.partial(kernel, zs),
        out_shape=jax.ShapeDtypeStruct((T, W), BF16),
        in_specs=[vmem] * 10 + [hbm] * 7,
        out_specs=vmem,
        scratch_shapes=scratch,
        compiler_params=pltpu.CompilerParams(
            collective_id=0, has_side_effects=True, vmem_limit_bytes=60 * 1024 * 1024
        ),
        name="layer",
    )(
        query_pre,
        forget_pre,
        values_in,
        gate_pre,
        floor_gap.reshape(1, W),
        head_gain.reshape(1, W),
        stream,
        norm_gain.reshape(1, W),
        route_ids.T,
        route_weights.T,
        out_proj,
        shared_gate,
        shared_up,
        shared_down,
        expert_gate.reshape(D, W),
        expert_up.reshape(D, W),
        expert_down.reshape(D, W),
    )


def solution(mesh):
    zs = mesh.shape["sp"] // 2
    finer = Mesh(mesh.devices.reshape(zs, 2, 4, 4), ("z", "c", "y", "x"))
    sp, tp = ("z", "c"), ("y", "x")
    in_specs = (
        P(sp, tp),
        P(sp, tp),
        P(sp, tp),
        P(sp, tp),
        P(tp),
        P(),
        P(sp, tp),
        P(None, tp),
        P(tp),
        P(sp, None),
        P(sp, None),
        P(sp, None, tp),
        P(sp, None, tp),
        P(sp, None, tp),
        P(None, tp),
        P(None, tp),
        P(None, tp),
    )
    return jax.shard_map(
        functools.partial(layer, zs),
        mesh=finer,
        in_specs=in_specs,
        out_specs=P(sp, tp),
        check_vma=False,
    )
```

time: 455 us -> 197 us (0.43)
  the two profiles are of different devices: /device:TPU:2 before, /device:TPU:1 now
where the time goes in v1:
time: 197 us
  Pallas kernels  195 us (99%)
    pallas_call x1, Pallas kernels, layer(): pl.pallas_call(functools.partial(kernel, zs), out_shape=jax.ShapeDtypeStr...  195 us

profile of v1, /device:TPU:1, one launch (start us, length us, event | category | flops | bytes accessed | tf_op | source)
XLA Modules:
  0.0 196.7 jit_solution(10047835542220703824)
XLA Ops:
  0.0 195.1 %layer.1 = bf16[512,128]{1,0:T(8,128)(2,1)} custom-call(bf16[512,128]{1,0:T(8,128)(2,1)} %query_ref.1, bf16[512,128]{1,0:T(8,128)(2,1)} %forget_ref.1, bf16[512,128]{1,0:T(8,128)(2,1)} %value_ref.1, bf16[512,128]{1,0:T(8,128)(2,1)} %gatep_ref.1, f32[1,128]{1,0:T(1,128)} %bitcast.13, f32[1,128]{1,0:T(1,128)} %bitcast.14, bf16[512,128]{1,0:T(8,128)(2,1)} %stream_ref.1, ...), custom_call_target="tpu_custom_call" | custom-call | tf_op jit(solution)/shard_map/layer/pallas_call | solution.py:607
  195.1 1.6 copy.19

commit v2 on v1

v2 whole, which is shorter than its diff:
```python
import functools

import jax
import jax.numpy as jnp
from jax import lax
from jax.experimental import pallas as pl
from jax.experimental.pallas import tpu as pltpu
from jax.sharding import Mesh
from jax.sharding import PartitionSpec as P

D = 2048
T = 512
W = 128
CAP = 64
EPS = 1e-06
MESH = pl.DeviceIdType.MESH
F32 = jnp.float32
BF16 = jnp.bfloat16


class Sems:
    def __init__(self):
        self.used = 0

    def take(self, count):
        first = self.used
        self.used += count
        return first


SEM = Sems()
CHUNKS = 2
CH = CAP // CHUNKS
INPUTS = SEM.take(17)
OUTPUT = SEM.take(1)
WEIGHTS = [SEM.take(5) for _ in range(3)]
PAIR = SEM.take(2)
PAIR_H = SEM.take(2)
NEAR_S, NEAR_R = SEM.take(8), SEM.take(8)
STATE_S, STATE_R = SEM.take(16), SEM.take(4)
DECAY_S, DECAY_R = SEM.take(16), SEM.take(4)
SQUARE = SEM.take(2)
OUT = [SEM.take(2) for _ in range(CHUNKS)]
BACK = [SEM.take(2) for _ in range(CHUNKS)]
ALONG_A = [SEM.take(4) for _ in range(3 + 2 * CHUNKS)]
ALONG_B = [SEM.take(17) for _ in range(3 + 2 * CHUNKS)]


def dot(left, right):
    return jnp.dot(left, right, preferred_element_type=F32)


def dot_last(left, right):
    return lax.dot_general(left, right, (((1,), (1,)), ((), ())), preferred_element_type=F32)


def dot_first(left, right):
    return lax.dot_general(left, right, (((0,), (0,)), ((), ())), preferred_element_type=F32)


def silu(v):
    return v * jax.nn.sigmoid(v)


def in_three(value):
    high = value.astype(BF16)
    rest = value - high.astype(F32)
    middle = rest.astype(BF16)
    low = (rest - middle.astype(F32)).astype(BF16)
    return high, middle, low


def diagonal():
    return lax.broadcasted_iota(jnp.int32, (W, W), 0) == lax.broadcasted_iota(jnp.int32, (W, W), 1)


def to_column(row):
    eye = diagonal()
    return jnp.concatenate(
        [
            jnp.sum(jnp.where(eye, row[:, k * W : (k + 1) * W], 0.0), axis=1, keepdims=True)
            for k in range(row.shape[1] // W)
        ],
        axis=0,
    )


def to_row(column):
    eye = diagonal()
    return jnp.concatenate(
        [
            jnp.sum(jnp.where(eye, column[k * W : (k + 1) * W], 0.0), axis=0, keepdims=True)
            for k in range(column.shape[0] // W)
        ],
        axis=1,
    )


def kernel(
    zs,
    forget_hbm,
    value_hbm,
    gap_hbm,
    query_hbm,
    gatep_hbm,
    head_gain_hbm,
    ids_hbm,
    eg_hbm,
    stream_hbm,
    norm_gain_hbm,
    weights_hbm,
    proj_hbm,
    eu_hbm,
    sg_hbm,
    su_hbm,
    sd_hbm,
    ed_hbm,
    out_hbm,
    forget_ref,
    value_ref,
    gap_ref,
    query_ref,
    gatep_ref,
    head_gain_ref,
    ids_ref,
    stream_ref,
    norm_gain_ref,
    weights_ref,
    out_ref,
    wo,
    wsg,
    wsu,
    wsd,
    weg,
    weu,
    wed,
    pair_mine,
    pair_other,
    near_send,
    near_recv,
    near_decay,
    near_decays,
    far_send,
    far_recv,
    far_decay,
    far_decays,
    half_mine,
    half_other,
    squares,
    x_mixed,
    x_normed,
    x_shared,
    x_rows,
    x_hidden,
    send_rows,
    recv_rows,
    result,
    gathered,
    back,
    choose,
    pick0,
    pick1,
    residual,
    total_out,
    within,
    carried,
    gate_act,
    slots,
    sems,
):
    z, c = lax.axis_index("z"), lax.axis_index("c")
    y, x = lax.axis_index("y"), lax.axis_index("x")
    me = z * 2 + c
    spn = zs * 2
    j = y * 4 + x
    a = x * (1 - c) + y * c
    b = y * (1 - c) + x * c
    chunk = spn * CH
    group = chunk // 4

    def plane(a_to, b_to):
        return (z, c, b_to * (1 - c) + a_to * c, a_to * (1 - c) + b_to * c)

    def number(a_to, b_to):
        return (b_to * (1 - c) + a_to * c) * 4 + a_to * (1 - c) + b_to * c

    def column(number_of):
        return pl.ds(pl.multiple_of(number_of * W, W), W)

    def rows_of(number_of, count, base=0):
        return pl.ds(pl.multiple_of(base + number_of * count, count), count)

    def remote(src, dst, sent, received, where):
        return pltpu.make_async_remote_copy(
            src_ref=src,
            dst_ref=dst,
            send_sem=sems.at[sent],
            recv_sem=sems.at[received],
            device_id=where,
            device_id_type=MESH,
        )

    local = {}
    for k, (name, src, dst) in enumerate(
        [
            ("forget", forget_hbm, forget_ref),
            ("gap", gap_hbm, gap_ref),
            ("value", value_hbm, value_ref),
            ("query", query_hbm, query_ref),
            ("gatep", gatep_hbm, gatep_ref),
            ("head", head_gain_hbm, head_gain_ref),
            ("ids", ids_hbm, ids_ref),
            ("eg", eg_hbm, weg.at[:, column(a)]),
            ("stream", stream_hbm, stream_ref),
            ("gain", norm_gain_hbm, norm_gain_ref),
            ("routes", weights_hbm, weights_ref),
            ("wo", proj_hbm, wo),
            ("eu", eu_hbm, weu.at[:, column(a)]),
            ("sg", sg_hbm, wsg),
            ("su", su_hbm, wsu),
            ("sd", sd_hbm, wsd),
            ("ed", ed_hbm, wed.at[:, column(a)]),
        ]
    ):
        local[name] = pltpu.make_async_copy(src, dst, sems.at[INPUTS + k])
        local[name].start()

    barrier = pltpu.get_barrier_semaphore()

    def greet_column(i, carry):
        to = (me + i) % spn
        pl.semaphore_signal(barrier, inc=1, device_id=(to // 2, to % 2, y, x), device_id_type=MESH)
        return carry

    def greet_plane(i, carry):
        to = (j + i) % 16
        pl.semaphore_signal(barrier, inc=1, device_id=(z, c, to // 4, to % 4), device_id_type=MESH)
        return carry

    lax.fori_loop(1, spn, greet_column, 0)
    lax.fori_loop(1, 16, greet_plane, 0)

    local["forget"].wait()
    local["gap"].wait()
    leakage = gap_ref[...] * jax.nn.sigmoid(-forget_ref[...].astype(F32))
    log_keep = jnp.log1p(-leakage)
    lower = (
        lax.broadcasted_iota(jnp.int32, (T, T), 0) >= lax.broadcasted_iota(jnp.int32, (T, T), 1)
    ).astype(BF16)
    high, middle, low = in_three(log_keep)
    growth = dot(lower, high) + dot(lower, middle) + dot(lower, low)
    closing = growth[T - 1 : T, :]
    local["value"].wait()
    values = value_ref[...]
    state = dot_first(values, (leakage * jnp.exp(closing - growth)).astype(BF16))
    through = jnp.exp(closing)
    pair_mine[0:W, :] = state
    pair_mine[W : W + 8, :] = jnp.broadcast_to(through, (8, W))

    pl.semaphore_wait(barrier, spn - 1 + 15)

    swap = remote(pair_mine, pair_other, PAIR, PAIR + 1, (z, 1 - c, y, x))
    swap.start()

    next_a, last_a = (a + 1) % 4, (a + 3) % 4
    pending = []

    def weight_copies(which, src, dst):
        sem = WEIGHTS[which]
        upper, lower_half, every = pl.ds(0, D // 2), pl.ds(D // 2, D // 2), pl.ds(0, D)

        def step(part, owner, to, kind, source=None):
            block = dst.at[part, column(owner)]
            return remote(source if source is not None else block, block, sem, sem + 1 + kind, plane(to, b))

        def begin():
            step(every, a, next_a, 0, src).start()
            step(every, a, last_a, 1, src).start()

        def forward():
            step(every, last_a, next_a, 0).wait_recv()
            step(upper, last_a, next_a, 2).start()
            step(every, next_a, last_a, 1).wait_recv()
            step(lower_half, next_a, last_a, 3).start()

        def finish():
            opposite = (a + 2) % 4
            step(upper, opposite, next_a, 2).wait_recv()
            step(lower_half, opposite, last_a, 3).wait_recv()
            sent = dst.at[:, pl.ds(0, 3 * W)]
            pending.append(remote(sent, sent, sem, sem + 1, plane(next_a, b)))

        return begin, forward, finish

    gate_begin, gate_forward, gate_finish = weight_copies(0, eg_hbm, weg)
    up_begin, up_forward, up_finish = weight_copies(1, eu_hbm, weu)
    down_begin, down_forward, down_finish = weight_copies(2, ed_hbm, wed)
    gate_begin()

    swap.wait_recv()
    other_state, other_through = pair_other[0:W, :], pair_other[W : W + 1, :]
    mine_first = c == 0
    first = jnp.where(mine_first, state, other_state)
    second = jnp.where(mine_first, other_state, state)
    second_through = jnp.where(mine_first, other_through, through)
    total = first * second_through + second
    mine_total = jnp.where(mine_first, total[0:CAP, :], total[CAP:W, :])
    mine_decay = through * other_through
    near_send[...] = mine_total.astype(BF16)
    near_decay[...] = mine_decay
    quad, spot = z // 4, z % 4

    def near_copies(to, slot):
        where = (quad * 4 + to, c, y, x)
        return (
            remote(near_send, near_recv.at[slot], NEAR_S + to, NEAR_R + slot, where),
            remote(near_decay, near_decays.at[slot], NEAR_S + 4 + to, NEAR_R + 4 + slot, where),
        )

    def far_copies(to, slot):
        where = (to, c, y, x)
        return (
            remote(far_send, far_recv.at[slot], STATE_S + to, STATE_R + slot, where),
            remote(far_decay, far_decays.at[slot], DECAY_S + to, DECAY_R + slot, where),
        )

    def send_near(to, carry):
        for copy in near_copies(to, spot):
            copy.start()
        return carry

    lax.fori_loop(spot + 1, 4, send_near, 0)

    local["query"].wait()
    local["gatep"].wait()
    local["head"].wait()
    queries = silu(query_ref[...].astype(F32))
    centre = growth[T // 2 - 1 : T // 2, :]
    scaled_q = (queries * jnp.exp(growth - centre)).astype(BF16)
    scaled_k = (leakage * jnp.exp(centre - growth)).astype(BF16)
    carried[...] = (queries * jnp.exp(growth)).astype(BF16)
    gate_act[...] = silu(gatep_ref[...].astype(F32)) * head_gain_ref[...]
    for k in range(T // W):
        upto = (k + 1) * W
        scores = dot_last(scaled_q[k * W : upto, :], scaled_k[0:upto, :])
        causal = lax.broadcasted_iota(jnp.int32, (W, upto), 0) + k * W >= lax.broadcasted_iota(
            jnp.int32, (W, upto), 1
        )
        scores = jnp.where(causal, scores, 0.0).astype(BF16)
        within[k * W : upto, :] = dot(scores, values[0:upto, :])

    local["ids"].wait()
    ids = ids_ref[...]
    lanes = lax.broadcasted_iota(jnp.int32, (W, T), 0)
    hits0, hits1 = lanes == ids[0:1, :], lanes == ids[1:2, :]
    before = (
        lax.broadcasted_iota(jnp.int32, (T, T), 0) < lax.broadcasted_iota(jnp.int32, (T, T), 1)
    ).astype(BF16)
    earlier = dot((hits0 | hits1).astype(BF16), before)
    place = earlier + lanes.astype(F32) * CH
    for h in range(1, CHUNKS):
        place += jnp.where(earlier >= h * CH, float(chunk - CH), 0.0)
    slot0 = jnp.sum(jnp.where(hits0, place, 0.0), axis=0, keepdims=True)
    slot1 = jnp.sum(jnp.where(hits1, place, 0.0), axis=0, keepdims=True)
    slots[0] = jnp.broadcast_to(to_column(slot0), (T, W))
    slots[1] = jnp.broadcast_to(to_column(slot1), (T, W))

    def build(i, carry):
        base = (i * W).astype(F32)
        down = lax.broadcasted_iota(jnp.int32, (W, T), 0).astype(F32) + base
        choose[rows_of(i, W), :] = ((down == slot0) | (down == slot1)).astype(BF16)
        along = lax.broadcasted_iota(jnp.int32, (T, W), 1).astype(F32) + base
        pick0[:, column(i)] = (slots[0] == along).astype(BF16)
        pick1[:, column(i)] = (slots[1] == along).astype(BF16)
        return carry

    lax.fori_loop(0, spn * CAP // W, build, 0)
    def take_near(k, held):
        for copy in near_copies(k, k):
            copy.wait_recv()
        return held[0] * near_decays[k] + near_recv[k].astype(F32), held[1] * near_decays[k]

    near, near_through = lax.fori_loop(
        0, spot, take_near, (jnp.zeros((CAP, W), F32), jnp.ones((1, W), F32))
    )
    far_send[...] = (near * near_decay[...] + mine_total).astype(BF16)
    far_decay[...] = near_through * near_decay[...]
    far_count = jnp.where(spot == 3, zs - 1 - z, 0)

    def send_far(i, carry):
        for copy in far_copies(zs - 1 - i, quad):
            copy.start()
        return carry

    lax.fori_loop(0, far_count, send_far, 0)
    gate_forward()
    up_begin()
    up_forward()

    def take_far(k, held):
        for copy in far_copies(k, k):
            copy.wait_recv()
        return held * far_decays[k] + far_recv[k].astype(F32)

    half = lax.fori_loop(0, quad, take_far, jnp.zeros((CAP, W), F32))
    half = half * near_through + near
    half_mine[...] = half
    swap_half = remote(half_mine, half_other, PAIR_H, PAIR_H + 1, (z, 1 - c, y, x))
    swap_half.start()
    swap_half.wait_recv()
    theirs = half_other[...]
    incoming = jnp.concatenate(
        [jnp.where(mine_first, half, theirs), jnp.where(mine_first, theirs, half)], axis=0
    )
    incoming = jnp.where(
        mine_first, incoming, incoming * pair_other[W : W + 1, :] + pair_other[0:W, :]
    )
    outputs = within[...] + dot_last(carried[...], incoming.astype(BF16))
    mean = jnp.mean(outputs * outputs, axis=1, keepdims=True)
    x_mixed[:, column(j)] = (outputs * lax.rsqrt(mean + EPS) * gate_act[...]).astype(BF16)

    def along_b(buffer, which, order):
        sem = ALONG_B[which]
        rows = buffer.shape[0]
        upper, lower_half, every = pl.ds(0, rows // 2), pl.ds(rows // 2, rows // 2), pl.ds(0, rows)
        right, left, opposite = (b + 1) % 4, (b + 3) % 4, (b + 2) % 4

        def step(i, part, b_of, to, kind):
            block = buffer.at[part, column(number((a + 4 - i) % 4, b_of))]
            return remote(block, block, sem, sem + 1 + 4 * kind + i, plane(a, to))

        def begin(i):
            step(i, every, b, right, 0).start()
            step(i, every, b, left, 1).start()

        def forward(i):
            step(i, every, left, right, 0).wait_recv()
            step(i, upper, left, right, 2).start()
            step(i, every, right, left, 1).wait_recv()
            step(i, lower_half, right, left, 3).start()

        def finish():
            for i in order:
                step(i, upper, opposite, right, 2).wait_recv()
                step(i, lower_half, opposite, left, 3).wait_recv()
            sent = buffer.at[:, pl.ds(0, 12 * W)]
            pending.append(remote(sent, sent, sem, sem + 1, plane(a, right)))

        return begin, forward, finish

    def send_along_a(which, source_of, target_of, from_block):
        sem = ALONG_A[which]
        for i in (1, 3, 2):
            to = (a + i) % 4
            remote(source_of(to), target_of(a), sem, sem + i, plane(to, b)).start()

        def ready(i):
            if i:
                block = target_of((a + 4 - i) % 4)
                remote(block, block, sem, sem + i, plane((a + i) % 4, b)).wait_recv()

        pending.append((sem, from_block))
        return ready

    def columns_of(buffer):
        return lambda number_a: buffer.at[:, column(number(number_a, b))]

    ORDER = (0, 1, 3, 2)

    def gather_begin(buffer, which):
        begin, forward, finish = along_b(buffer, which, ORDER)
        own = buffer.at[:, column(j)]
        ready = send_along_a(which, lambda to: own, columns_of(buffer), buffer.at[:, pl.ds(0, 3 * W)])
        begin(0)

        def rest():
            last = 0
            for i in ORDER[1:]:
                ready(i)
                begin(i)
                forward(last)
                last = i
            forward(last)

        return rest, finish

    mixed_rest, mixed_finish = gather_begin(x_mixed, 0)
    mixed_rest()
    mixed_finish()

    local["wo"].wait()
    local["stream"].wait()
    res = stream_ref[...].astype(F32) + dot(x_mixed[...], wo[...])
    residual[...] = res
    squares[j] = to_row(jnp.sum(res * res, axis=1, keepdims=True))

    def send_squares(i, carry):
        to = (j + i) % 16
        remote(squares.at[j], squares.at[j], SQUARE, SQUARE + 1, (z, c, to // 4, to % 4)).start()
        return carry

    lax.fori_loop(1, 16, send_squares, 0)
    fifteen = squares.at[pl.ds(0, 15)]
    all_squares = remote(fifteen, fifteen, SQUARE, SQUARE + 1, plane(next_a, b))
    all_squares.wait_recv()
    summed = jnp.sum(squares[...], axis=0)
    scale = to_column(lax.rsqrt(summed / D + EPS))
    local["gain"].wait()
    normed = (res * scale * norm_gain_ref[...]).astype(BF16)
    x_normed[:, column(j)] = normed

    def exchange(src, dst, pair, h):
        def send(i, carry):
            to = (me + i) % spn
            remote(
                src.at[rows_of(to, CH, h * chunk), :],
                dst.at[rows_of(me, CH, h * chunk), :],
                pair,
                pair + 1,
                (to // 2, to % 2, y, x),
            ).start()
            return carry

        lax.fori_loop(1, spn, send, 0)
        dst[rows_of(me, CH, h * chunk), :] = src[rows_of(me, CH, h * chunk), :]
        others = dst.at[pl.ds(h * chunk, chunk - CH), :]
        whole = remote(others, others, pair, pair + 1, (z, 1 - c, y, x))
        pending.append(whole)
        return whole.wait_recv

    arrived = []
    for h in range(CHUNKS):
        for k in range(chunk // T):
            part = slice(h * chunk + k * T, h * chunk + (k + 1) * T)
            send_rows[part, :] = dot(choose[part, :], normed).astype(BF16)
        arrived.append(exchange(send_rows, recv_rows, OUT[h], h))

    def rows_start(h):
        arrived[h]()
        own_rows = rows_of(a, group, h * chunk)
        x_rows[h, :, column(j)] = recv_rows[own_rows, :]
        return send_along_a(
            3 + h,
            lambda to: recv_rows.at[rows_of(to, group, h * chunk), :],
            columns_of(x_rows.at[h]),
            x_rows.at[h, :, pl.ds(0, 3 * W)],
        )

    def gate_up(h):
        step = min(group, 2 * W)
        for k in range(group // step):
            part = slice(k * step, (k + 1) * step)
            rows_in = x_rows[h, part, :]
            hidden = (silu(dot(rows_in, weg[...])) * dot(rows_in, weu[...])).astype(BF16)
            for n in range(4):
                x_hidden[h, part, column(number(n, b))] = hidden[:, n * W : (n + 1) * W]

    def down_back(h):
        step = min(group, 2 * W)
        for k in range(group // step):
            part = slice(k * step, (k + 1) * step)
            rows_out = dot(x_hidden[h, part, :], wed[...]).astype(BF16)
            for n in range(4):
                result[h, n, part, :] = rows_out[:, n * W : (n + 1) * W]
        ready = send_along_a(
            3 + CHUNKS + h,
            lambda to: result.at[h, to],
            lambda number_a: gathered.at[rows_of(number_a, group, h * chunk), :],
            gathered.at[pl.ds(h * chunk, 3 * group), :],
        )
        gathered[rows_of(a, group, h * chunk), :] = result[h, a]
        return ready

    rows_b = [along_b(x_rows.at[h], 3 + h, ORDER) for h in range(CHUNKS)]
    hidden_b = [along_b(x_hidden.at[h], 3 + CHUNKS + h, ORDER) for h in range(CHUNKS)]

    def rows_begin(h, ready):
        for i in ORDER:
            ready(i)
            rows_b[h][0](i)

    def each(function):
        for i in ORDER:
            function(i)

    def go_back(h, ready):
        for i in (1, 3, 2):
            ready(i)
        return exchange(gathered, back, BACK[h], h)

    normed_rest, normed_finish = gather_begin(x_normed, 1)
    normed_rest()
    ready0 = rows_start(0)
    down_begin()
    normed_finish()
    local["sg"].wait()
    local["su"].wait()
    hidden = silu(dot(x_normed[...], wsg[...])) * dot(x_normed[...], wsu[...])
    x_shared[:, column(j)] = hidden.astype(BF16)
    rows_begin(0, ready0)
    each(rows_b[0][1])
    down_forward()
    rows_b[0][2]()
    gate_finish()
    local["eg"].wait()
    up_finish()
    local["eu"].wait()
    gate_up(0)
    each(hidden_b[0][0])
    ready1 = rows_start(1)
    each(hidden_b[0][1])
    rows_begin(1, ready1)
    hidden_b[0][2]()
    down_finish()
    local["ed"].wait()
    back0 = down_back(0)
    each(rows_b[1][1])
    returned0 = go_back(0, back0)
    rows_b[1][2]()
    gate_up(1)
    each(hidden_b[1][0])
    shared_rest, shared_finish = gather_begin(x_shared, 2)
    each(hidden_b[1][1])
    hidden_b[1][2]()
    back1 = down_back(1)
    returned1 = go_back(1, back1)
    shared_rest()
    shared_finish()
    local["sd"].wait()
    local["routes"].wait()
    weights = weights_ref[...]
    weight0, weight1 = to_column(weights[0:1, :]), to_column(weights[1:2, :])
    total_out[...] = residual[...] + dot(x_shared[...], wsd[...])

    def routed(h):
        part = slice(h * chunk, (h + 1) * chunk)
        rows_in = back[part, :]
        return dot(pick0[:, part], rows_in) * weight0 + dot(pick1[:, part], rows_in) * weight1

    returned0()
    total_out[...] += routed(0)

    swap.wait_send()
    swap_half.wait_send()
    all_squares.wait_send()

    def drain_near(to, carry):
        for copy in near_copies(to, spot):
            copy.wait_send()
        return carry

    def drain_far(i, carry):
        for copy in far_copies(zs - 1 - i, quad):
            copy.wait_send()
        return carry

    lax.fori_loop(spot + 1, 4, drain_near, 0)
    lax.fori_loop(0, far_count, drain_far, 0)
    for item in pending:
        if isinstance(item, tuple):
            item = remote(item[1], item[1], item[0], item[0] + 1, plane(next_a, b))
        item.wait_send()

    returned1()
    out_ref[...] = (total_out[...] + routed(1)).astype(BF16)
    leave = pltpu.make_async_copy(out_ref, out_hbm, sems.at[OUTPUT])
    leave.start()
    leave.wait()


def layer(zs, *args):
    (
        query_pre,
        forget_pre,
        values_in,
        gate_pre,
        floor_gap,
        head_gain,
        stream,
        out_proj,
        norm_gain,
        route_ids,
        route_weights,
        expert_gate,
        expert_up,
        expert_down,
        shared_gate,
        shared_up,
        shared_down,
    ) = args
    rows = zs * 2 * CAP
    group = rows // (4 * CHUNKS)
    hbm = pl.BlockSpec(memory_space=pl.ANY)
    tokens = pltpu.VMEM((T, W), BF16)
    line = pltpu.VMEM((1, W), F32)
    scratch = [
        tokens,
        tokens,
        line,
        tokens,
        tokens,
        line,
        pltpu.VMEM((2, T), jnp.int32),
        tokens,
        line,
        pltpu.VMEM((2, T), F32),
        tokens,
        *[pltpu.VMEM((D, W), BF16)] * 4,
        *[pltpu.VMEM((D, 4 * W), BF16)] * 3,
        *[pltpu.VMEM((W + 8, W), F32)] * 2,
        *[
            pltpu.VMEM((CAP, W), BF16),
            pltpu.VMEM((4, CAP, W), BF16),
            line,
            pltpu.VMEM((4, 1, W), F32),
        ]
        * 2,
        *[pltpu.VMEM((CAP, W), F32)] * 2,
        pltpu.VMEM((16, 1, T), F32),
        *[pltpu.VMEM((T, D), BF16)] * 3,
        *[pltpu.VMEM((CHUNKS, group, D), BF16)] * 2,
        *[pltpu.VMEM((rows, W), BF16)] * 2,
        pltpu.VMEM((CHUNKS, 4, group, W), BF16),
        *[pltpu.VMEM((rows, W), BF16)] * 2,
        pltpu.VMEM((rows, T), BF16),
        *[pltpu.VMEM((T, rows), BF16)] * 2,
        *[pltpu.VMEM((T, W), F32)] * 3,
        tokens,
        pltpu.VMEM((T, W), F32),
        pltpu.VMEM((2, T, W), F32),
        pltpu.SemaphoreType.DMA((SEM.used,)),
    ]
    return pl.pallas_call(
        functools.partial(kernel, zs),
        out_shape=jax.ShapeDtypeStruct((T, W), BF16),
        in_specs=[hbm] * 17,
        out_specs=hbm,
        scratch_shapes=scratch,
        compiler_params=pltpu.CompilerParams(
            collective_id=0, has_side_effects=True, vmem_limit_bytes=60 * 1024 * 1024
        ),
        name="layer",
    )(
        forget_pre,
        values_in,
        floor_gap.reshape(1, W),
        query_pre,
        gate_pre,
        head_gain.reshape(1, W),
        route_ids.T,
        expert_gate.reshape(D, W),
        stream,
        norm_gain.reshape(1, W),
        route_weights.T,
        out_proj,
        expert_up.reshape(D, W),
        shared_gate,
        shared_up,
        shared_down,
        expert_down.reshape(D, W),
    )


def solution(mesh):
    zs = mesh.shape["sp"] // 2
    finer = Mesh(mesh.devices.reshape(zs, 2, 4, 4), ("z", "c", "y", "x"))
    sp, tp = ("z", "c"), ("y", "x")
    in_specs = (
        P(sp, tp),
        P(sp, tp),
        P(sp, tp),
        P(sp, tp),
        P(tp),
        P(),
        P(sp, tp),
        P(None, tp),
        P(tp),
        P(sp, None),
        P(sp, None),
        P(sp, None, tp),
        P(sp, None, tp),
        P(sp, None, tp),
        P(None, tp),
        P(None, tp),
        P(None, tp),
    )
    return jax.shard_map(
        functools.partial(layer, zs),
        mesh=finer,
        in_specs=in_specs,
        out_specs=P(sp, tp),
        check_vma=False,
    )
```

time: 197 us -> 159 us (0.81)
  the two profiles are of different devices: /device:TPU:1 before, /device:TPU:8 now
where the time goes in v2:
time: 159 us
  Pallas kernels  157 us (99%)
    pallas_call x1, Pallas kernels, layer(): pl.pallas_call(functools.partial(kernel, zs), out_shape=jax.ShapeDtypeStr...  157 us

profile of v2, /device:TPU:8, one launch (start us, length us, event | category | flops | bytes accessed | tf_op | source)
XLA Modules:
  0.0 158.8 jit_solution(10867628758430423187)
XLA Ops:
  0.0 157.2 %layer.1 = bf16[512,128]{1,0:T(8,128)(2,1)} custom-call(bf16[512,128]{1,0:T(8,128)(2,1)} %forget_hbm.1, bf16[512,128]{1,0:T(8,128)(2,1)} %value_hbm.1, f32[1,128]{1,0:T(1,128)} %bitcast.13, bf16[512,128]{1,0:T(8,128)(2,1)} %query_hbm.1, bf16[512,128]{1,0:T(8,128)(2,1)} %gatep_hbm.1, f32[1,128]{1,0:T(1,128)} %bitcast.14, s32[2,512]{1,0:T(2,128)} %bitcast.11, ...), custom_call_target="tpu_custom_call" | custom-call | tf_op jit(solution)/shard_map/layer/pallas_call | solution.py:733
  157.2 1.6 copy.19

commit v3 on v2

--- a/solution.py
+++ b/solution.py
@@ -29,19 +29,22 @@
 
 
 SEM = Sems()
-CHUNKS = 2
+CHUNKS = 4
+SPACING = 1
 CH = CAP // CHUNKS
 INPUTS = SEM.take(17)
 OUTPUT = SEM.take(1)
-WEIGHTS = [SEM.take(5) for _ in range(3)]
+WEIGHTS = [SEM.take(13) for _ in range(3)]
 PAIR = SEM.take(2)
 PAIR_H = SEM.take(2)
 NEAR_S, NEAR_R = SEM.take(8), SEM.take(8)
 STATE_S, STATE_R = SEM.take(16), SEM.take(4)
 DECAY_S, DECAY_R = SEM.take(16), SEM.take(4)
 SQUARE = SEM.take(2)
+SCALE = SEM.take(2)
 OUT = [SEM.take(2) for _ in range(CHUNKS)]
 BACK = [SEM.take(2) for _ in range(CHUNKS)]
+RING_A = [SEM.take(5) for _ in range(3)]
 ALONG_A = [SEM.take(4) for _ in range(3 + 2 * CHUNKS)]
 ALONG_B = [SEM.take(17) for _ in range(3 + 2 * CHUNKS)]
 
@@ -166,6 +169,9 @@
     carried,
     gate_act,
     slots,
+    ranks,
+    scales_send,
+    scales_recv,
     sems,
 ):
     z, c = lax.axis_index("z"), lax.axis_index("c")
@@ -264,29 +270,35 @@
 
     next_a, last_a = (a + 1) % 4, (a + 3) % 4
     pending = []
+    PIECES = 4
 
     def weight_copies(which, src, dst):
         sem = WEIGHTS[which]
-        upper, lower_half, every = pl.ds(0, D // 2), pl.ds(D // 2, D // 2), pl.ds(0, D)
-
-        def step(part, owner, to, kind, source=None):
+
+        def step(k, owner, to, slot, source=None):
+            part = pl.ds(k * (D // PIECES), D // PIECES)
             block = dst.at[part, column(owner)]
-            return remote(source if source is not None else block, block, sem, sem + 1 + kind, plane(to, b))
-
-        def begin():
-            step(every, a, next_a, 0, src).start()
-            step(every, a, last_a, 1, src).start()
-
-        def forward():
-            step(every, last_a, next_a, 0).wait_recv()
-            step(upper, last_a, next_a, 2).start()
-            step(every, next_a, last_a, 1).wait_recv()
-            step(lower_half, next_a, last_a, 3).start()
+            return remote(
+                block if source is None else source.at[part, :], block, sem, sem + 1 + slot, plane(to, b)
+            )
+
+        def begin(*pieces):
+            for k in pieces:
+                step(k, a, next_a, k, src).start()
+                step(k, a, last_a, 4 + k, src).start()
+
+        def forward(*pieces):
+            for k in pieces:
+                owner, to, slot = (last_a, next_a, k) if k % 2 == 0 else (next_a, last_a, 4 + k)
+                step(k, owner, to, slot).wait_recv()
+                step(k, owner, to, 8 + k).start()
 
         def finish():
             opposite = (a + 2) % 4
-            step(upper, opposite, next_a, 2).wait_recv()
-            step(lower_half, opposite, last_a, 3).wait_recv()
+            for k in range(PIECES):
+                owner, to, slot = (next_a, last_a, 4 + k) if k % 2 == 0 else (last_a, next_a, k)
+                step(k, owner, to, slot).wait_recv()
+                step(k, opposite, owner, 8 + k).wait_recv()
             sent = dst.at[:, pl.ds(0, 3 * W)]
             pending.append(remote(sent, sent, sem, sem + 1, plane(next_a, b)))
 
@@ -295,7 +307,7 @@
     gate_begin, gate_forward, gate_finish = weight_copies(0, eg_hbm, weg)
     up_begin, up_forward, up_finish = weight_copies(1, eu_hbm, weu)
     down_begin, down_forward, down_finish = weight_copies(2, ed_hbm, wed)
-    gate_begin()
+    gate_begin(0, 1, 2, 3)
 
     swap.wait_recv()
     other_state, other_through = pair_other[0:W, :], pair_other[W : W + 1, :]
@@ -362,6 +374,10 @@
         place += jnp.where(earlier >= h * CH, float(chunk - CH), 0.0)
     slot0 = jnp.sum(jnp.where(hits0, place, 0.0), axis=0, keepdims=True)
     slot1 = jnp.sum(jnp.where(hits1, place, 0.0), axis=0, keepdims=True)
+    among = lax.broadcasted_iota(jnp.int32, (T, W), 1).astype(F32)
+    for k, hits in enumerate((hits0, hits1)):
+        rank = jnp.sum(jnp.where(hits, earlier, 0.0), axis=0, keepdims=True)
+        ranks[k] = (to_column(rank) == among).astype(BF16)
     slots[0] = jnp.broadcast_to(to_column(slot0), (T, W))
     slots[1] = jnp.broadcast_to(to_column(slot1), (T, W))
 
@@ -393,9 +409,8 @@
         return carry
 
     lax.fori_loop(0, far_count, send_far, 0)
-    gate_forward()
-    up_begin()
-    up_forward()
+    gate_forward(0, 1, 2, 3)
+    up_begin(0, 1)
 
     def take_far(k, held):
         for copy in far_copies(k, k):
@@ -469,24 +484,42 @@
 
     def gather_begin(buffer, which):
         begin, forward, finish = along_b(buffer, which, ORDER)
-        own = buffer.at[:, column(j)]
-        ready = send_along_a(which, lambda to: own, columns_of(buffer), buffer.at[:, pl.ds(0, 3 * W)])
+        sem = RING_A[which]
+        upper, lower_half, every = pl.ds(0, T // 2), pl.ds(T // 2, T // 2), pl.ds(0, T)
+
+        def step(part, owner, to, kind):
+            block = buffer.at[part, column(number(owner, b))]
+            return remote(block, block, sem, sem + 1 + kind, plane(to, b))
+
+        step(every, a, next_a, 0).start()
+        step(every, a, last_a, 1).start()
         begin(0)
 
-        def rest():
-            last = 0
-            for i in ORDER[1:]:
-                ready(i)
-                begin(i)
-                forward(last)
-                last = i
-            forward(last)
-
-        return rest, finish
-
-    mixed_rest, mixed_finish = gather_begin(x_mixed, 0)
-    mixed_rest()
-    mixed_finish()
+        def first():
+            step(every, last_a, next_a, 0).wait_recv()
+            step(upper, last_a, next_a, 2).start()
+            begin(1)
+            step(every, next_a, last_a, 1).wait_recv()
+            step(lower_half, next_a, last_a, 3).start()
+            begin(3)
+
+        def second():
+            forward(0)
+            opposite = (a + 2) % 4
+            step(upper, opposite, next_a, 2).wait_recv()
+            step(lower_half, opposite, last_a, 3).wait_recv()
+            begin(2)
+
+        def third():
+            forward(1)
+            forward(3)
+            forward(2)
+            pending.append((sem, buffer.at[:, pl.ds(0, 3 * W)]))
+
+        return first, second, third, finish
+
+    for part in gather_begin(x_mixed, 0):
+        part()
 
     local["wo"].wait()
     local["stream"].wait()
@@ -500,18 +533,14 @@
         return carry
 
     lax.fori_loop(1, 16, send_squares, 0)
-    fifteen = squares.at[pl.ds(0, 15)]
-    all_squares = remote(fifteen, fifteen, SQUARE, SQUARE + 1, plane(next_a, b))
-    all_squares.wait_recv()
-    summed = jnp.sum(squares[...], axis=0)
-    scale = to_column(lax.rsqrt(summed / D + EPS))
     local["gain"].wait()
-    normed = (res * scale * norm_gain_ref[...]).astype(BF16)
+    normed = (res * norm_gain_ref[...]).astype(BF16)
     x_normed[:, column(j)] = normed
+    up_begin(2, 3)
 
     def exchange(src, dst, pair, h):
-        def send(i, carry):
-            to = (me + i) % spn
+        def send(n, carry):
+            to = (me + spn // 2 + (n + 1) // 2 * (n % 2 * 2 - 1)) % spn
             remote(
                 src.at[rows_of(to, CH, h * chunk), :],
                 dst.at[rows_of(me, CH, h * chunk), :],
@@ -521,7 +550,7 @@
             ).start()
             return carry
 
-        lax.fori_loop(1, spn, send, 0)
+        lax.fori_loop(0, spn - 1, send, 0)
         dst[rows_of(me, CH, h * chunk), :] = src[rows_of(me, CH, h * chunk), :]
         others = dst.at[pl.ds(h * chunk, chunk - CH), :]
         whole = remote(others, others, pair, pair + 1, (z, 1 - c, y, x))
@@ -529,11 +558,64 @@
         return whole.wait_recv
 
     arrived = []
-    for h in range(CHUNKS):
-        for k in range(chunk // T):
-            part = slice(h * chunk + k * T, h * chunk + (k + 1) * T)
-            send_rows[part, :] = dot(choose[part, :], normed).astype(BF16)
+
+    def dispatch(h):
+        part = slice(h * chunk, (h + 1) * chunk)
+        send_rows[part, :] = dot(choose[part, :], normed).astype(BF16)
         arrived.append(exchange(send_rows, recv_rows, OUT[h], h))
+
+    dispatch(0)
+
+    fifteen = squares.at[pl.ds(0, 15)]
+    all_squares = remote(fifteen, fifteen, SQUARE, SQUARE + 1, plane(next_a, b))
+    all_squares.wait_recv()
+    factor = lax.rsqrt(jnp.sum(squares[...], axis=0) / D + EPS)
+    experts = lax.broadcasted_iota(jnp.int32, (spn, T), 0)
+    by_rank = jnp.zeros((spn, W), F32)
+    for k in range(2):
+        for piece in in_three(jnp.where(experts == ids_ref[k : k + 1, :], factor, 0.0)):
+            by_rank += dot(piece, ranks[k])
+    for k in range(spn):
+        scales_send[k] = by_rank[k : k + 1, :]
+
+    def send_scales(i, carry):
+        to = (me + i) % spn
+        remote(
+            scales_send.at[to], scales_recv.at[me], SCALE, SCALE + 1, (to // 2, to % 2, y, x)
+        ).start()
+        return carry
+
+    lax.fori_loop(1, spn, send_scales, 0)
+    scales_recv[me] = scales_send[me]
+    others = scales_recv.at[pl.ds(0, spn - 1)]
+    all_scales = remote(others, others, SCALE, SCALE + 1, (z, 1 - c, y, x))
+    pending.append(all_scales)
+    dispatch(1)
+
+    up_forward(0, 1, 2, 3)
+    dispatch(2)
+    dispatch(3)
+    down_begin(0, 1)
+    scale = to_column(factor)
+    local["routes"].wait()
+    weights = weights_ref[...]
+    weight0, weight1 = to_column(weights[0:1, :]), to_column(weights[1:2, :])
+    side = []
+
+    def normed_start():
+        side[0:0] = gather_begin(x_normed, 1)
+
+    side.append(normed_start)
+
+    def shared_hidden():
+        local["sg"].wait()
+        local["su"].wait()
+        rows_in = x_normed[...]
+        hidden = silu(dot(rows_in, wsg[...]) * scale) * (dot(rows_in, wsu[...]) * scale)
+        x_shared[:, column(j)] = hidden.astype(BF16)
+        side.extend(gather_begin(x_shared, 2))
+
+    side.append(shared_hidden)
 
     def rows_start(h):
         arrived[h]()
@@ -547,13 +629,22 @@
         )
 
     def gate_up(h):
-        step = min(group, 2 * W)
-        for k in range(group // step):
-            part = slice(k * step, (k + 1) * step)
-            rows_in = x_rows[h, part, :]
-            hidden = (silu(dot(rows_in, weg[...])) * dot(rows_in, weu[...])).astype(BF16)
-            for n in range(4):
-                x_hidden[h, part, column(number(n, b))] = hidden[:, n * W : (n + 1) * W]
+        lane = lax.broadcasted_iota(jnp.int32, (CH, W), 1)
+        place_of = lax.broadcasted_iota(jnp.int32, (CH, W), 0) + h * CH
+        factors = jnp.concatenate(
+            [
+                jnp.sum(
+                    jnp.where(lane == place_of, scales_recv[a * (spn // 4) + k], 0.0), axis=1, keepdims=True
+                )
+                for k in range(spn // 4)
+            ],
+            axis=0,
+        )
+        rows_in = x_rows[h]
+        hidden = silu(dot(rows_in, weg[...]) * factors) * (dot(rows_in, weu[...]) * factors)
+        hidden = hidden.astype(BF16)
+        for n in range(4):
+            x_hidden[h, :, column(number(n, b))] = hidden[:, n * W : (n + 1) * W]
 
     def down_back(h):
         step = min(group, 2 * W)
@@ -588,48 +679,61 @@
             ready(i)
         return exchange(gathered, back, BACK[h], h)
 
-    normed_rest, normed_finish = gather_begin(x_normed, 1)
-    normed_rest()
-    ready0 = rows_start(0)
-    down_begin()
-    normed_finish()
-    local["sg"].wait()
-    local["su"].wait()
-    hidden = silu(dot(x_normed[...], wsg[...])) * dot(x_normed[...], wsu[...])
-    x_shared[:, column(j)] = hidden.astype(BF16)
-    rows_begin(0, ready0)
-    each(rows_b[0][1])
-    down_forward()
-    rows_b[0][2]()
-    gate_finish()
-    local["eg"].wait()
-    up_finish()
-    local["eu"].wait()
-    gate_up(0)
-    each(hidden_b[0][0])
-    ready1 = rows_start(1)
-    each(hidden_b[0][1])
-    rows_begin(1, ready1)
-    hidden_b[0][2]()
-    down_finish()
-    local["ed"].wait()
-    back0 = down_back(0)
-    each(rows_b[1][1])
-    returned0 = go_back(0, back0)
-    rows_b[1][2]()
-    gate_up(1)
-    each(hidden_b[1][0])
-    shared_rest, shared_finish = gather_begin(x_shared, 2)
-    each(hidden_b[1][1])
-    hidden_b[1][2]()
-    back1 = down_back(1)
-    returned1 = go_back(1, back1)
-    shared_rest()
-    shared_finish()
+    held = {}
+
+    def start_rows(h):
+        held[h] = rows_start(h)
+        if h == 0:
+            down_begin(2)
+
+    def begin_rows(h):
+        rows_begin(h, held[h])
+        if h == 0:
+            down_begin(3)
+            down_forward(0, 1)
+
+    def forward_rows(h):
+        each(rows_b[h][1])
+        if h == 0:
+            down_forward(2, 3)
+
+    def through_gate(h):
+        rows_b[h][2]()
+        if h == 0:
+            gate_finish()
+            local["eg"].wait()
+            up_finish()
+            local["eu"].wait()
+            all_scales.wait_recv()
+        gate_up(h)
+        each(hidden_b[h][0])
+
+    def forward_hidden(h):
+        each(hidden_b[h][1])
+
+    def through_down(h):
+        hidden_b[h][2]()
+        if h == 0:
+            down_finish()
+            local["ed"].wait()
+        held[h] = down_back(h)
+
+    def send_home(h):
+        held[h] = go_back(h, held[h])
+
+    steps = (start_rows, begin_rows, forward_rows, through_gate, forward_hidden, through_down, send_home)
+    SIDE = (2, 4, 5, 6, 7, 8)
+    for tick in range(SPACING * (CHUNKS - 1) + len(steps)):
+        for h in range(CHUNKS):
+            at = tick - SPACING * h
+            if 0 <= at < len(steps):
+                steps[at](h)
+        for _ in range(SIDE.count(tick)):
+            side.pop(0)()
+
+    while side:
+        side.pop(0)()
     local["sd"].wait()
-    local["routes"].wait()
-    weights = weights_ref[...]
-    weight0, weight1 = to_column(weights[0:1, :]), to_column(weights[1:2, :])
     total_out[...] = residual[...] + dot(x_shared[...], wsd[...])
 
     def routed(h):
@@ -637,8 +741,9 @@
         rows_in = back[part, :]
         return dot(pick0[:, part], rows_in) * weight0 + dot(pick1[:, part], rows_in) * weight1
 
-    returned0()
-    total_out[...] += routed(0)
+    for h in range(CHUNKS - 1):
+        held[h]()
+        total_out[...] += routed(h)
 
     swap.wait_send()
     swap_half.wait_send()
@@ -661,8 +766,8 @@
             item = remote(item[1], item[1], item[0], item[0] + 1, plane(next_a, b))
         item.wait_send()
 
-    returned1()
-    out_ref[...] = (total_out[...] + routed(1)).astype(BF16)
+    held[CHUNKS - 1]()
+    out_ref[...] = (total_out[...] + routed(CHUNKS - 1)).astype(BF16)
     leave = pltpu.make_async_copy(out_ref, out_hbm, sems.at[OUTPUT])
     leave.start()
     leave.wait()
@@ -728,6 +833,8 @@
         tokens,
         pltpu.VMEM((T, W), F32),
         pltpu.VMEM((2, T, W), F32),
+        pltpu.VMEM((2, T, W), BF16),
+        *[pltpu.VMEM((zs * 2, 1, W), F32)] * 2,
         pltpu.SemaphoreType.DMA((SEM.used,)),
     ]
     return pl.pallas_call(

time: 159 us -> 135 us (0.85)
  Pallas kernels: 157 us -> 133 us
    pallas_call x1, Pallas kernels: 157 us -> 133 us  [layer(): pl.pallas_call(functools.partial(kernel, zs), out_shape=jax.ShapeDtypeStr...]
where the time goes in v3:
time: 135 us
  Pallas kernels  133 us (99%)
  local copies, waits for them, and re-layouts  1.57 us (1%)
    pallas_call x1, Pallas kernels, layer(): pl.pallas_call(functools.partial(kernel, zs), out_shape=jax.ShapeDtypeStr...  133 us

profile of v3, /device:TPU:8, one launch (start us, length us, event | category | flops | bytes accessed | tf_op | source)
XLA Modules:
  0.0 134.9 jit_solution(15144910182420677221)
XLA Ops:
  0.0 133.3 %layer.1 = bf16[512,128]{1,0:T(8,128)(2,1)} custom-call(bf16[512,128]{1,0:T(8,128)(2,1)} %forget_hbm.1, bf16[512,128]{1,0:T(8,128)(2,1)} %value_hbm.1, f32[1,128]{1,0:T(1,128)} %bitcast.13, bf16[512,128]{1,0:T(8,128)(2,1)} %query_hbm.1, bf16[512,128]{1,0:T(8,128)(2,1)} %gatep_hbm.1, f32[1,128]{1,0:T(1,128)} %bitcast.14, s32[2,512]{1,0:T(2,128)} %bitcast.11, ...), custom_call_target="tpu_custom_call" | custom-call | tf_op jit(solution)/shard_map/layer/pallas_call | solution.py:840
  133.3 1.6 %copy.19 = bf16[512,128]{1,0:T(8,128)(2,1)} copy(bf16[512,128]{1,0:T(8,128)(2,1)} %layer.1) | data formatting | bytes 262144

commit v4 on v3

--- a/solution.py
+++ b/solution.py
@@ -536,6 +536,7 @@
     local["gain"].wait()
     normed = (res * norm_gain_ref[...]).astype(BF16)
     x_normed[:, column(j)] = normed
+    normed_parts = list(gather_begin(x_normed, 1))
     up_begin(2, 3)
 
     def exchange(src, dst, pair, h):
@@ -592,20 +593,17 @@
     pending.append(all_scales)
     dispatch(1)
 
+    normed_parts.pop(0)()
     up_forward(0, 1, 2, 3)
     dispatch(2)
     dispatch(3)
+    normed_parts.pop(0)()
     down_begin(0, 1)
     scale = to_column(factor)
     local["routes"].wait()
     weights = weights_ref[...]
     weight0, weight1 = to_column(weights[0:1, :]), to_column(weights[1:2, :])
-    side = []
-
-    def normed_start():
-        side[0:0] = gather_begin(x_normed, 1)
-
-    side.append(normed_start)
+    side = normed_parts
 
     def shared_hidden():
         local["sg"].wait()
@@ -722,7 +720,7 @@
         held[h] = go_back(h, held[h])
 
     steps = (start_rows, begin_rows, forward_rows, through_gate, forward_hidden, through_down, send_home)
-    SIDE = (2, 4, 5, 6, 7, 8)
+    SIDE = (1, 2, 7, 8, 9)
     for tick in range(SPACING * (CHUNKS - 1) + len(steps)):
         for h in range(CHUNKS):
             at = tick - SPACING * h

time: 135 us -> 136 us (level)
  no operation moved by 1% of the time
where the time goes in v4:
time: 136 us
  Pallas kernels  134 us (99%)
  local copies, waits for them, and re-layouts  1.57 us (1%)
    pallas_call x1, Pallas kernels, layer(): pl.pallas_call(functools.partial(kernel, zs), out_shape=jax.ShapeDtypeStr...  134 us

profile of v4, /device:TPU:8, one launch (start us, length us, event | category | flops | bytes accessed | tf_op | source)
XLA Modules:
  0.0 135.8 jit_solution(15981088332524398644)
XLA Ops:
  0.0 134.2 %layer.1 = bf16[512,128]{1,0:T(8,128)(2,1)} custom-call(bf16[512,128]{1,0:T(8,128)(2,1)} %forget_hbm.1, bf16[512,128]{1,0:T(8,128)(2,1)} %value_hbm.1, f32[1,128]{1,0:T(1,128)} %bitcast.13, bf16[512,128]{1,0:T(8,128)(2,1)} %query_hbm.1, bf16[512,128]{1,0:T(8,128)(2,1)} %gatep_hbm.1, f32[1,128]{1,0:T(1,128)} %bitcast.14, s32[2,512]{1,0:T(2,128)} %bitcast.11, ...), custom_call_target="tpu_custom_call" | custom-call | tf_op jit(solution)/shard_map/layer/pallas_call | solution.py:838
  134.2 1.6 %copy.19 = bf16[512,128]{1,0:T(8,128)(2,1)} copy(bf16[512,128]{1,0:T(8,128)(2,1)} %layer.1) | data formatting | bytes 262144
